TPU v7x, 128 devices: a whole 4x4x4 slice. The times are simulated.
128 devices in a mesh: sp: 32 (over z, y, core), tp: 4 (over x).
Axes of the slice: x: 4, y: 4, z: 4, core: 2. Of those that a mesh axis runs over, the one named last changes fastest.
Arguments:
- residual_in: bfloat16 [65536, 2048], P(('sp', 'tp')), may hold values from -6 to 6
- conv_input: bfloat16 [65536, 1024], P('sp', 'tp'), may hold values from -6 to 6
- input_gate: bfloat16 [65536, 1024], P('sp', 'tp'), may hold values from -6 to 6
- output_gate: bfloat16 [65536, 1024], P('sp', 'tp'), may hold values from -6 to 6
- conv_taps: bfloat16 [3, 1024], P(None, 'tp'), may hold values from -3.5 to 3.5
- doc_ids: int32 [65536], P('sp'), may hold values from 0 to 15, never falling along the last dimension, each value on 1 to 8192 neighbouring positions
- proj_weight: bfloat16 [1024, 2048], replicated, may hold values from -0.1875 to 0.1875
- norm_gain: float32 [2048], replicated, may hold values from 0.1 to 1.9
- expert_ids: int32 [65536, 2], P(('sp', 'tp')), may hold values from 0 to 31, all different within a row; in each aligned block of 512 rows (0 to 511, 512 to 1023, ...) at most 64 rows name the same one
- expert_weight: float32 [65536, 2], P(('sp', 'tp')), may hold values from 0.05 to 1
- w_gate: bfloat16 [32, 2048, 512], P('sp'), may hold values from -0.125 to 0.125
- w_up: bfloat16 [32, 2048, 512], P('sp'), may hold values from -0.125 to 0.125
- w_down: bfloat16 [32, 512, 2048], P('sp'), may hold values from -0.25 to 0.25
Outputs:
- layer_out: bfloat16 [65536, 2048], P(('sp', 'tp'))
Inputs may be any that keep to these rules, and one draw needn't show every extreme that they name: `doc_ids`: numbers never fall along the sequence; one document spans at most 8192 positions. `expert_ids`: a token's two experts differ; in each aligned block of rows that one device holds, no expert is named more than 64 times, a bound that some block reaches.
All inputs are finite; a program needn't handle non-finite values.
Results may differ from a plain program's by a relative error of at most 0.0047.
Values may be sent and summed in bfloat16 or wider, within the bound.
A program may use at most 128 MiB of HBM per device.

v0:
```python
import jax
import jax.numpy as jnp
from jax import lax
from jax.sharding import PartitionSpec as P

EXPERTS = 32
CAP = 64


epsilon = 1e-06


def from_behind(x, axis, by):
    devices = lax.axis_size(axis)
    pairs = [(i, i + by) for i in range(devices) if 0 <= i + by < devices]
    return lax.ppermute(x, axis, pairs)


def per_device(
    residual_in,
    conv_input,
    input_gate,
    output_gate,
    conv_taps,
    doc_ids,
    proj_weight,
    norm_gain,
    expert_ids,
    expert_weight,
    w_gate,
    w_up,
    w_down,
):
    kernel_width = conv_taps.shape[0]
    rim_rows = kernel_width - 1
    product = input_gate.astype(jnp.float32) * conv_input.astype(jnp.float32)
    doc_float = doc_ids.astype(jnp.float32)
    prev_in, prev_ids = from_behind((product[-rim_rows:], doc_float[-rim_rows:]), "sp", 1)
    padded_in = jnp.concatenate([prev_in, product], axis=0)
    padded_ids = jnp.concatenate([prev_ids, doc_float], axis=0)
    length = product.shape[0]
    conv_sum = jnp.zeros(product.shape, jnp.float32)
    for offset in range(kernel_width):
        same_doc = padded_ids[offset : offset + length] == doc_float
        term = conv_taps[offset].astype(jnp.float32)[None, :] * padded_in[offset : offset + length]
        conv_sum = conv_sum + jnp.where(same_doc[:, None], term, 0.0)
    gated = (output_gate.astype(jnp.float32) * conv_sum).astype(jnp.bfloat16)
    regrouped = lax.all_to_all(gated, "tp", split_axis=0, concat_axis=1, tiled=True)
    mixed = jnp.dot(regrouped, proj_weight, preferred_element_type=jnp.float32)
    hidden = residual_in.astype(jnp.float32) + mixed
    scale_rows = lax.rsqrt(jnp.mean(hidden * hidden, axis=-1, keepdims=True) + epsilon)
    normed = (hidden * scale_rows * norm_gain[None, :]).astype(jnp.bfloat16)
    local_experts = w_gate.shape[0]
    model_width = normed.shape[1]
    flat_ids = expert_ids.reshape(-1)
    one_hot = (flat_ids[:, None] == jnp.arange(EXPERTS, dtype=jnp.int32)[None, :]).astype(jnp.int32)
    before = jnp.cumsum(one_hot, axis=0) - one_hot
    slot_index = flat_ids * CAP + jnp.sum(before * one_hot, axis=1)
    source_rows = jnp.repeat(normed, 2, axis=0)
    buffer = jnp.zeros((EXPERTS * CAP, model_width), jnp.bfloat16).at[slot_index].set(source_rows)
    buffer = buffer.reshape(lax.axis_size("sp"), local_experts, CAP, model_width)
    slots = lax.all_to_all(buffer, "sp", split_axis=0, concat_axis=0, tiled=True)
    gate_val = jnp.einsum("aend,edf->aenf", slots, w_gate, preferred_element_type=jnp.float32)
    up_val = jnp.einsum("aend,edf->aenf", slots, w_up, preferred_element_type=jnp.float32)
    act_rows = (jax.nn.silu(gate_val) * up_val).astype(jnp.bfloat16)
    expert_out = jnp.einsum(
        "aenf,efd->aend", act_rows, w_down, preferred_element_type=jnp.float32
    ).astype(jnp.bfloat16)
    returned = lax.all_to_all(expert_out, "sp", split_axis=0, concat_axis=0, tiled=True).reshape(
        EXPERTS * CAP, model_width
    )
    picked = returned[slot_index].astype(jnp.float32) * expert_weight.reshape(-1)[:, None]
    expert_sum = jnp.sum(picked.reshape(-1, 2, model_width), axis=1)
    return (hidden + expert_sum).astype(jnp.bfloat16)


def solution(mesh):
    return jax.shard_map(
        per_device,
        mesh=mesh,
        in_specs=(
            P(("sp", "tp"), None),
            P("sp", "tp"),
            P("sp", "tp"),
            P("sp", "tp"),
            P(None, "tp"),
            P("sp"),
            P(),
            P(),
            P(("sp", "tp"), None),
            P(("sp", "tp"), None),
            P("sp", None, None),
            P("sp", None, None),
            P("sp", None, None),
        ),
        out_specs=P(("sp", "tp"), None),
        check_vma=False,
    )
```

profile of v0, /device:TPU:0, one launch (start us, length us, event | category | flops | bytes accessed | tf_op | source)
XLA Modules:
  0.0 357.5 jit_solution(186289497554102982)
XLA Ops:
  0.9 1.3 collective-permute-start
  2.2 1.8 convert_multiply_fusion
  4.0 1.3 copy-done.4
  5.3 4.3 %collective-permute-start.1 = (f32[2,256]{1,0:T(2,128)S(1)}, f32[2,256]{1,0:T(2,128)S(1)}, u32[]{:S(2)}, u32[]{:S(2)}) collective-permute-start(f32[2,256]{1,0:T(2,128)S(1)} %slice.49), channel_id=1, source_target_pairs={{0,4},{4,8},{8,12},{12,16},{16,20},{20,24},{24,28},{28,32},{32,36}... | collective-permute-start | bytes 6152 | tf_op jit(solution)/shard_map/ppermute | solution.py:16
  10.8 9.0 %reduce-window.6 = s32[32,8,128]{2,1,0:T(8,128)S(1)} reduce-window(s32[32,8,128]{2,1,0:T(8,128)S(1)} %fusion.36, s32[]{:T(128)} %constant.6.clone.1), window={size=1x1x128 pad=0_0x0_0x127_0}, to_apply=%region_0.1 | reduce-window | flops 4161536 | bytes 262148 | tf_op jit(solution)/shard_map/reduce-window
  20.2 5.9 %fusion.18 = bf16[2048,256]{1,0:T(8,128)(2,1)} fusion(f32[2,256]{1,0:T(2,128)S(1)} %collective-permute-done.1, f32[2048,256]{1,0:T(8,128)} %copy-done.4, bf16[2048,256]{1,0:T(8,128)(2,1)} %param.16, f32[256]{0:T(256)S(1)} %bitcast.111, f32[256]{0:T(256)S(1)} %bitcast.112, f32[256]{0:T(256)S(1)} %bitcast.110, pred[2048]{0:T(1024)(128)(4,1)S(1)} %convert_compare_fusion, ...), kind=kLoop, calls=%fused_computation.29 | loop fusion | flops 6815744 | bytes 4205568 | tf_op jit(solution)/shard_map/convert_element_type | solution.py:47
  26.1 4.3 %all-to-all-start = ((bf16[4,512,256]{2,1,0:T(8,128)(2,1)}), bf16[4,512,256]{2,1,0:T(8,128)(2,1)S(1)}, u32[]{:S(2)}, u32[]{:S(2)}) async-start(bf16[4,512,256]{2,1,0:T(8,128)(2,1)} %bitcast.104), calls=%async_computation | async-start | bytes 2097152 | tf_op jit(solution)/shard_map/all_to_all | solution.py:48
  34.2 11.6 %all-to-all-done = bf16[4,512,256]{2,1,0:T(8,128)(2,1)S(1)} async-done(((bf16[4,512,256]{2,1,0:T(8,128)(2,1)}), bf16[4,512,256]{2,1,0:T(8,128)(2,1)S(1)}, u32[]{:S(2)}, u32[]{:S(2)}) %all-to-all-start) | async-done | bytes 1048608 | tf_op jit(solution)/shard_map/all_to_all | solution.py:48
  46.7 1.5 copy.28
  48.2 5.5 %multiply_reduce_fusion.1 = (f32[512]{0:T(512)S(1)}, f32[512,2048]{1,0:T(8,128)S(1)}) fusion(bf16[512,1024]{0,1:T(8,128)(2,1)S(1)} %bitcast.102, bf16[1024,2048]{1,0:T(8,128)(2,1)} %param.19, bf16[512,2048]{1,0:T(8,128)(2,1)} %param.13), kind=kOutput, calls=%fused_computation.17 | convolution fusion | flops 2151677440 | bytes 11536384 | tf_op jit(solution)/shard_map/dot_general | solution.py:49
  53.8 1.9 copy-done.2
  56.1 3.8 %broadcast_in_dim.46 = bf16[512,2,2048]{2,1,0:T(2,128)(2,1)} broadcast(bf16[512,2048]{1,0:T(8,128)(2,1)S(1)} %multiply_convert_fusion), dimensions={0,2} | broadcast | bytes 6291456 | tf_op jit(solution)/shard_map/broadcast_in_dim | solution.py:59
  59.9 7.2 %reshape.125 = bf16[1024,2048]{1,0:T(8,128)(2,1)} reshape(bf16[512,2,2048]{2,1,0:T(2,128)(2,1)} %broadcast_in_dim.46) | data formatting | bytes 8388608 | tf_op jit(solution)/shard_map/reshape | solution.py:59
  67.0 12.3 %scatter_custom_fusion = bf16[2048,2048]{1,0:T(8,128)(2,1)} fusion(s32[1024]{0:T(1024)S(1)} %bitcast.108, bf16[1024,2048]{1,0:T(8,128)(2,1)} %reshape.125, bf16[]{:T(256)} %constant.5.clone.1), kind=kCustom, calls=%fused_computation.18 | custom fusion | bytes 8389120 | tf_op jit(solution)/shard_map/scatter | solution.py:60
  79.3 104.0 %all_to_all.29 = bf16[32,1,64,2048]{3,2,1,0:T(8,128)(2,1)S(1)} all-to-all(bf16[32,1,64,2048]{3,2,1,0:T(8,128)(2,1)} %bitcast.101), channel_id=1, replica_groups=mesh['sp'=32,'tp'=4] {'sp'}, dimensions={0} | all-to-all | bytes 16777216 | tf_op jit(solution)/shard_map/all_to_all | solution.py:62
  183.4 3.2 copy-done.5
  186.6 6.0 %fusion = f32[32,64,512]{2,1,0:T(8,128)} fusion(bf16[32,1,64,2048]{3,2,1,0:T(8,128)(2,1)S(1)} %all_to_all.29, bf16[1,2048,512]{2,1,0:T(8,128)(2,1)S(1)} %copy-done.12), kind=kOutput, calls=%fused_computation.2 | convolution fusion | flops 4294967296 | bytes 14680064 | tf_op jit(solution)/shard_map/aend,edf->aenf/dot_general | solution.py:64
  192.6 14.8 %convert_bitcast_fusion = bf16[32,1,64,2048]{3,2,1,0:T(8,128)(2,1)} fusion(bf16[1,512,2048]{2,1,0:T(8,128)(2,1)S(1)} %copy-done, f32[32,64,512]{2,1,0:T(8,128)} %fusion, bf16[32,1,64,2048]{3,2,1,0:T(8,128)(2,1)} %copy-done.5, bf16[1,2048,512]{2,1,0:T(8,128)(2,1)} %param.23), kind=kOutput, calls=%fused_computation.7 | convolution fusion | flops 8600420352 | bytes 25165824 | tf_op jit(solution)/shard_map/aenf,efd->aend/dot_general | solution.py:66
  207.4 5.3 %all-to-all-start.2 = ((bf16[32,1,64,2048]{3,2,1,0:T(8,128)(2,1)}), bf16[32,1,64,2048]{3,2,1,0:T(8,128)(2,1)}, u32[]{:S(2)}, u32[]{:S(2)}) async-start(bf16[32,1,64,2048]{3,2,1,0:T(8,128)(2,1)} %convert_bitcast_fusion), calls=%async_computation.2 | async-start | bytes 16777216 | tf_op jit(solution)/shard_map/all_to_all | solution.py:69
  212.9 105.5 %all-to-all-done.2 = bf16[32,1,64,2048]{3,2,1,0:T(8,128)(2,1)} async-done(((bf16[32,1,64,2048]{3,2,1,0:T(8,128)(2,1)}), bf16[32,1,64,2048]{3,2,1,0:T(8,128)(2,1)}, u32[]{:S(2)}, u32[]{:S(2)}) %all-to-all-start.2) | async-done | bytes 8388640 | tf_op jit(solution)/shard_map/all_to_all | solution.py:69
  318.4 13.3 %gather_fusion = bf16[1024,2048]{1,0:T(8,128)(2,1)} fusion(bf16[2048,2048]{1,0:T(8,128)(2,1)} %bitcast.31, s32[1024]{0:T(1024)S(1)} %broadcast_clamp_fusion), kind=kCustom, calls=%fused_computation | custom fusion | bytes 8392704 | tf_op jit(solution)/shard_map/gather | solution.py:72
  331.7 9.7 %reshape.112 = f32[512,2,2048]{2,1,0:T(2,128)} reshape(bf16[1024,2048]{1,0:T(8,128)(2,1)} %gather_fusion) | data formatting | bytes 12582912 | tf_op jit(solution)/shard_map/convert_element_type | solution.py:72
  341.4 14.2 %multiply_reduce_fusion = f32[512,2048]{1,0:T(8,128)S(1)} fusion(f32[512,2,2048]{2,1,0:T(2,128)} %reshape.112, f32[512,2]{1,0:T(8,128)S(1)} %copy.35), kind=kLoop, calls=%fused_computation.6 | loop fusion | flops 3145728 | bytes 12587008 | tf_op jit(solution)/shard_map/reduce_sum | solution.py:73
  355.6 1.9 add_convert_fusion
  (50 shorter events, 7.7 us)
Async XLA Ops:
  0.0 192.6 %copy-start = (bf16[1,512,2048]{2,1,0:T(8,128)(2,1)S(1)}, bf16[1,512,2048]{2,1,0:T(8,128)(2,1)}, u32[]{:S(2)}) copy-start(bf16[1,512,2048]{2,1,0:T(8,128)(2,1)} %param.25) | copy-start | bytes 6291460
  0.0 9.7 %copy-start.7 = (s32[2048]{0:T(1024)S(1)}, s32[2048]{0:T(1024)}, u32[]{:S(2)}) copy-start(s32[2048]{0:T(1024)} %param.18) | copy-start | bytes 24580
  0.0 9.7 %copy-start.8 = (s32[512,2]{0,1:T(2,128)S(1)}, s32[512,2]{0,1:T(2,128)}, u32[]{:S(2)}) copy-start(s32[512,2]{0,1:T(2,128)} %param.21) | copy-start | bytes 12292
  0.0 10.8 %copy-start.10 = (bf16[3,256]{1,0:T(4,128)(2,1)S(1)}, bf16[3,256]{1,0:T(4,128)(2,1)}, u32[]{:S(2)}) copy-start(bf16[3,256]{1,0:T(4,128)(2,1)} %param.17) | copy-start | bytes 4612
  0.9 19.2 %collective-permute-start = (f32[2]{0:T(128)S(1)}, f32[2]{0:T(128)S(1)}, u32[]{:S(2)}, u32[]{:S(2)}) collective-permute-start(f32[2]{0:T(128)S(1)} %slice.46), channel_id=1, source_target_pairs={{0,4},{4,8},{8,12},{12,16},{16,20},{20,24},{24,28},{28,32},{32,36}... | collective-permute-start | bytes 32 | tf_op jit(solution)/shard_map/ppermute | solution.py:16
  4.0 1.3 copy-start.4
  5.3 14.9 %collective-permute-start.1 = (f32[2,256]{1,0:T(2,128)S(1)}, f32[2,256]{1,0:T(2,128)S(1)}, u32[]{:S(2)}, u32[]{:S(2)}) collective-permute-start(f32[2,256]{1,0:T(2,128)S(1)} %slice.49), channel_id=1, source_target_pairs={{0,4},{4,8},{8,12},{12,16},{16,20},{20,24},{24,28},{28,32},{32,36}... | collective-permute-start | bytes 6152 | tf_op jit(solution)/shard_map/ppermute | solution.py:16
  26.1 19.6 %all-to-all-start = ((bf16[4,512,256]{2,1,0:T(8,128)(2,1)}), bf16[4,512,256]{2,1,0:T(8,128)(2,1)S(1)}, u32[]{:S(2)}, u32[]{:S(2)}) async-start(bf16[4,512,256]{2,1,0:T(8,128)(2,1)} %bitcast.104), calls=%async_computation | async-start | bytes 2097152 | tf_op jit(solution)/shard_map/all_to_all | solution.py:48
  45.7 1.0 copy-start.6
  48.2 7.5 %copy-start.9 = (f32[2048]{0:T(1024)S(1)}, f32[2048]{0:T(1024)}, u32[]{:S(2)}) copy-start(f32[2048]{0:T(1024)} %param.20) | copy-start | bytes 24580
  53.7 1.9 copy-start.2
  79.3 107.2 %copy-start.12 = (bf16[1,2048,512]{2,1,0:T(8,128)(2,1)S(1)}, bf16[1,2048,512]{2,1,0:T(8,128)(2,1)}, u32[]{:S(2)}) copy-start(bf16[1,2048,512]{2,1,0:T(8,128)(2,1)} %param.24) | copy-start | bytes 6291460
  183.4 3.2 copy-start.5
  207.4 5.4 %copy-start.11 = (f32[512,2]{0,1:T(2,128)S(1)}, f32[512,2]{0,1:T(2,128)}, u32[]{:S(2)}) copy-start(f32[512,2]{0,1:T(2,128)} %param.22) | copy-start | bytes 12292
  207.4 111.0 %all-to-all-start.2 = ((bf16[32,1,64,2048]{3,2,1,0:T(8,128)(2,1)}), bf16[32,1,64,2048]{3,2,1,0:T(8,128)(2,1)}, u32[]{:S(2)}, u32[]{:S(2)}) async-start(bf16[32,1,64,2048]{3,2,1,0:T(8,128)(2,1)} %convert_bitcast_fusion), calls=%async_computation.2 | async-start | bytes 16777216 | tf_op jit(solution)/shard_map/all_to_all | solution.py:69
  341.4 14.2 %copy-start.3 = (f32[512,2048]{1,0:T(8,128)S(1)}, f32[512,2048]{1,0:T(8,128)}, u32[]{:S(2)}) copy-start(f32[512,2048]{1,0:T(8,128)} %copy-done.2) | copy-start | bytes 12582916
  341.4 16.1 %copy-start.1 = (bf16[1,512,2048]{2,1,0:T(8,128)(2,1)S(1)}, bf16[1,512,2048]{2,1,0:T(8,128)(2,1)}, u32[]{:S(2)}) copy-start(bf16[1,512,2048]{2,1,0:T(8,128)(2,1)} %param.25) | copy-start | bytes 6291460
where the time goes:
time: 358 us
  waiting for transfers between devices  117 us (33%)
  blocking collectives  104 us (29%)
  local copies, waits for them, and re-layouts  58.4 us (16%)
  other arithmetic  36.3 us (10%)
  matrix products  26.3 us (7%)
  starting transfers between devices  15.2 us (4%)
    all_to_all x1, waiting for transfers between devices, per_device(): lax.all_to_all(expert_out, 'sp', split_axis=0, concat_axis=0, tiled=True)  105 us
    all_to_all x1, blocking collectives, per_device(): lax.all_to_all(buffer, 'sp', split_axis=0, concat_axis=0, tiled=True)  104 us
    dot_general x1, matrix products, per_device(): jnp.einsum('aenf,efd->aend', act_rows, w_down, preferred_element_type=jnp...  14.8 us
    reduce_sum x1, other arithmetic, per_device(): expert_sum = jnp.sum(picked.reshape(-1, 2, model_width), axis=1)  14.2 us
    gather x1, local copies, waits for them, and re-layouts, per_device(): returned[slot_index].astype(jnp.float32)  13.3 us
    scatter x1, local copies, waits for them, and re-layouts, per_device(): jnp.zeros((EXPERTS * CAP, model_width), jnp.bfloat16).at[slot_index]  12.3 us
    all_to_all x1, waiting for transfers between devices, per_device(): lax.all_to_all(gated, 'tp', split_axis=0, concat_axis=1, tiled=True)  11.6 us
    convert_element_type x1, local copies, waits for them, and re-layouts, per_device(): returned[slot_index].astype(jnp.float32)  9.68 us
  transfers between devices with their start and end apart: 4, of which 2 were waited for; matrix products, arithmetic and copies ran while one was open for 5% of the time, Pallas kernels for 0%

commit v1 on v0

v1 whole, which is shorter than its diff:
```python
import jax
import jax.numpy as jnp
from jax import lax
from jax.sharding import PartitionSpec as P

EXPERTS = 32
CAP = 64
epsilon = 1e-06
F32 = jnp.float32
BF16 = jnp.bfloat16


def from_behind(x, axis, by):
    devices = lax.axis_size(axis)
    pairs = [(i, i + by) for i in range(devices) if 0 <= i + by < devices]
    return lax.ppermute(x, axis, pairs)


def per_device(
    residual_in,
    conv_input,
    input_gate,
    output_gate,
    conv_taps,
    doc_ids,
    proj_weight,
    norm_gain,
    expert_ids,
    expert_weight,
    w_gate,
    w_up,
    w_down,
):
    kernel_width = conv_taps.shape[0]
    rim = kernel_width - 1
    length, channels = conv_input.shape
    doc_float = doc_ids.astype(F32)
    tail = input_gate[-rim:].astype(F32) * conv_input[-rim:].astype(F32)
    packed = jnp.concatenate([tail, jnp.broadcast_to(doc_float[-rim:, None], (rim, 128))], axis=1)
    prev = from_behind(packed, "sp", 1)
    prev_in, prev_ids = prev[:, :channels], prev[:, channels]
    first = lax.axis_index("sp") == 0
    prev_ids = jnp.where(first, -1.0, prev_ids)
    product = input_gate.astype(F32) * conv_input.astype(F32)
    padded_in = jnp.concatenate([prev_in, product], axis=0)
    padded_ids = jnp.concatenate([prev_ids, doc_float], axis=0)
    conv_sum = jnp.zeros(product.shape, F32)
    for offset in range(kernel_width):
        same_doc = padded_ids[offset : offset + length] == doc_float
        term = conv_taps[offset].astype(F32)[None, :] * padded_in[offset : offset + length]
        conv_sum = conv_sum + jnp.where(same_doc[:, None], term, 0.0)
    gated = (output_gate.astype(F32) * conv_sum).astype(BF16)
    regrouped = lax.all_to_all(gated, "tp", split_axis=0, concat_axis=1, tiled=True)

    tokens = expert_ids.shape[0]
    experts = jnp.arange(EXPERTS, dtype=jnp.int32)
    ids_t = expert_ids.T
    weight_t = expert_weight.T
    hit = [ids_t[j][None, :] == experts[:, None] for j in range(2)]
    used = hit[0] | hit[1]
    weight_of = jnp.where(hit[0], weight_t[0][None, :], 0.0) + jnp.where(hit[1], weight_t[1][None, :], 0.0)
    t_row = lax.broadcasted_iota(jnp.int32, (tokens, tokens), 0)
    t_col = lax.broadcasted_iota(jnp.int32, (tokens, tokens), 1)
    earlier = (t_row < t_col).astype(BF16)
    rank = jnp.dot(used.astype(BF16), earlier, preferred_element_type=F32)
    code = jnp.where(used, rank, -1.0)
    slot_of = lax.broadcasted_iota(jnp.int32, (EXPERTS, CAP, tokens), 1).astype(F32)
    match = code[:, None, :] == slot_of
    dispatch = match.astype(BF16).reshape(EXPERTS * CAP, tokens)
    combine = jnp.where(match, weight_of[:, None, :], 0.0).astype(BF16).reshape(EXPERTS * CAP, tokens)

    mixed = jnp.dot(regrouped, proj_weight, preferred_element_type=F32)
    hidden = residual_in.astype(F32) + mixed
    scale_rows = lax.rsqrt(jnp.mean(hidden * hidden, axis=-1, keepdims=True) + epsilon)
    normed = (hidden * scale_rows * norm_gain[None, :]).astype(BF16)
    width = normed.shape[1]
    buffer = jnp.dot(dispatch, normed, preferred_element_type=F32).astype(BF16)
    buffer = buffer.reshape(EXPERTS, CAP, width)
    slots = lax.all_to_all(buffer, "sp", split_axis=0, concat_axis=0, tiled=True).reshape(EXPERTS * CAP, width)
    gate_val = jnp.dot(slots, w_gate[0], preferred_element_type=F32)
    up_val = jnp.dot(slots, w_up[0], preferred_element_type=F32)
    act_rows = (jax.nn.silu(gate_val) * up_val).astype(BF16)
    expert_out = jnp.dot(act_rows, w_down[0], preferred_element_type=F32).astype(BF16)
    expert_out = expert_out.reshape(EXPERTS, CAP, width)
    returned = lax.all_to_all(expert_out, "sp", split_axis=0, concat_axis=0, tiled=True).reshape(EXPERTS * CAP, width)
    expert_sum = lax.dot_general(combine, returned, (((0,), (0,)), ((), ())), preferred_element_type=F32)
    return (hidden + expert_sum).astype(BF16)


def solution(mesh):
    return jax.shard_map(
        per_device,
        mesh=mesh,
        in_specs=(
            P(("sp", "tp"), None),
            P("sp", "tp"),
            P("sp", "tp"),
            P("sp", "tp"),
            P(None, "tp"),
            P("sp"),
            P(),
            P(),
            P(("sp", "tp"), None),
            P(("sp", "tp"), None),
            P("sp", None, None),
            P("sp", None, None),
            P("sp", None, None),
        ),
        out_specs=P(("sp", "tp"), None),
        check_vma=False,
    )
```

time: 358 us -> 289 us (0.81)
  local copies, waits for them, and re-layouts: 58.4 us -> 2.74 us
  other arithmetic: 36.3 us -> 12.4 us
  matrix products: 26.3 us -> 37.4 us
  starting transfers between devices: 15.2 us -> 11.5 us
    reduce_sum x2 -> x0, other arithmetic: 14.9 us -> none  [the longest x1 14.2 us: per_device(): expert_sum = jnp.sum(picked.reshape(-1, 2, model_width), axis=1)]
    gather x1 -> x0, local copies, waits for them, and re-layouts: 13.3 us -> none  [per_device(): returned[slot_index].astype(jnp.float32)]
    scatter x1 -> x0, local copies, waits for them, and re-layouts: 12.3 us -> none  [per_device(): jnp.zeros((EXPERTS * CAP, model_width), jnp.bfloat16).at[slot_index]]
    dot_general x3 -> x7, matrix products: 26.3 us -> 37.4 us  [the longest x1 9.88 us: per_device(): lax.dot_general(combine, returned, (((0,), (0,)), ((), ())), preferred_el...]
    convert_element_type x1 -> x0, local copies, waits for them, and re-layouts: 9.68 us -> none  [per_device(): returned[slot_index].astype(jnp.float32)]
    another operation x3 -> x0, other arithmetic: 9.14 us -> none
    reshape x1 -> x0, local copies, waits for them, and re-layouts: 7.19 us -> none  [per_device(): source_rows = jnp.repeat(normed, 2, axis=0)]
    unnamed x28 -> x24, local copies, waits for them, and re-layouts: 7.74 us -> 1.02 us
  transfers between devices with their start and end apart: 4 -> 3, of which waited for: 2 -> 2; matrix products, arithmetic and copies ran while one was open for 5% -> 2% of each run, Pallas kernels for 0% -> 0%
where the time goes in v1:
time: 289 us
  waiting for transfers between devices  120 us (42%)
  blocking collectives  105 us (36%)
  matrix products  37.4 us (13%)
  other arithmetic  12.4 us (4%)
  starting transfers between devices  11.5 us (4%)
    all_to_all x1, waiting for transfers between devices, per_device(): lax.all_to_all(expert_out, 'sp', split_axis=0, concat_axis=0, tiled=True)  106 us
    all_to_all x1, blocking collectives, per_device(): lax.all_to_all(buffer, 'sp', split_axis=0, concat_axis=0, tiled=True)  105 us
    all_to_all x1, waiting for transfers between devices, per_device(): lax.all_to_all(gated, 'tp', split_axis=0, concat_axis=1, tiled=True)  14 us
    dot_general x1, matrix products, per_device(): lax.dot_general(combine, returned, (((0,), (0,)), ((), ())), preferred_el...  9.88 us
    dot_general x1, matrix products, per_device(): jnp.dot(act_rows, w_down[0], preferred_element_type=F32).astype(BF16)  6.74 us
    convert_element_type x1, other arithmetic, per_device(): gated = (output_gate.astype(F32) * conv_sum).astype(BF16)  5.9 us
    dot_general x1, matrix products, per_device(): mixed = jnp.dot(regrouped, proj_weight, preferred_element_type=F32)  5.8 us
  transfers between devices with their start and end apart: 3, of which 2 were waited for; matrix products, arithmetic and copies ran while one was open for 2% of the time, Pallas kernels for 0%

profile of v1, /device:TPU:0, one launch (start us, length us, event | category | flops | bytes accessed | tf_op | source)
XLA Modules:
  0.0 288.9 jit_solution(236948942608263788)
XLA Ops:
  0.0 0.8 convert_element_type.61
  0.9 0.1 slice.64
  0.9 0.7 convert_multiply_fusion.1
  1.7 1.4 collective-permute-start
  3.2 3.1 %convert_multiply_fusion = f32[2048,256]{1,0:T(8,128)} fusion(bf16[2048,256]{1,0:T(8,128)(2,1)} %param.14, bf16[2048,256]{1,0:T(8,128)(2,1)} %param.15), kind=kLoop, calls=%fused_computation.31 | loop fusion | flops 1572864 | bytes 4194304 | tf_op jit(solution)/shard_map/mul | solution.py:44
  6.3 0.1 fusion.27
  6.4 0.1 fusion.25
  6.5 5.9 %fusion.7 = bf16[2048,256]{1,0:T(8,128)(2,1)} fusion(f32[2,256]{1,0:T(2,128)S(1)} %slice.68, f32[2048,256]{1,0:T(8,128)} %convert_multiply_fusion, bf16[2048,256]{1,0:T(8,128)(2,1)S(1)} %copy-done.4, f32[256]{0:T(256)S(1)} %bitcast.51, f32[256]{0:T(256)S(1)} %bitcast.52, f32[256]{0:T(256)S(1)} %bitcast.50, pred[2048]{0:T(1024)(128)(4,1)S(1)} %convert_compare_fusion, ...), kind=kLoop, calls=%fused_computation.18 | loop fusion | flops 6815744 | bytes 4205568 | tf_op jit(solution)/shard_map/convert_element_type | solution.py:52
  12.4 5.0 %all-to-all-start = ((bf16[4,512,256]{2,1,0:T(8,128)(2,1)}), bf16[4,512,256]{2,1,0:T(8,128)(2,1)S(1)}, u32[]{:S(2)}, u32[]{:S(2)}) async-start(bf16[4,512,256]{2,1,0:T(8,128)(2,1)} %bitcast.43), calls=%async_computation | async-start | bytes 2097152 | tf_op jit(solution)/shard_map/all_to_all | solution.py:53
  17.4 0.1 iota.41
  17.5 0.2 convolution_select_fusion
  17.7 1.6 bitcast_compare_fusion
  19.3 14.0 %all-to-all-done = bf16[4,512,256]{2,1,0:T(8,128)(2,1)S(1)} async-done(((bf16[4,512,256]{2,1,0:T(8,128)(2,1)}), bf16[4,512,256]{2,1,0:T(8,128)(2,1)S(1)}, u32[]{:S(2)}, u32[]{:S(2)}) %all-to-all-start) | async-done | bytes 1048608 | tf_op jit(solution)/shard_map/all_to_all | solution.py:53
  33.3 1.0 copy-done.2
  34.3 1.5 copy.15
  35.8 5.8 %multiply_reduce_fusion = (f32[512]{0:T(512)S(1)}, f32[512,2048]{1,0:T(8,128)S(1)}) fusion(bf16[512,1024]{0,1:T(8,128)(2,1)S(1)} %bitcast.41, bf16[1024,2048]{1,0:T(8,128)(2,1)} %param.19, bf16[512,2048]{1,0:T(8,128)(2,1)} %param.13), kind=kOutput, calls=%fused_computation.7 | convolution fusion | flops 2151677440 | bytes 11536384 | tf_op jit(solution)/shard_map/dot_general | solution.py:72
  41.6 5.1 %convolution_convert_fusion.1 = bf16[2048,2048]{1,0:T(8,128)(2,1)S(1)} fusion(pred[2048,512]{1,0:T(32,128)(4,1)S(1)} %copy-done.3, f32[512,2048]{1,0:T(8,128)S(1)} %get-tuple-element.15, f32[2048]{0:T(1024)S(1)} %copy-done.11, f32[512]{0:T(512)S(1)} %add_rsqrt_fusion), kind=kOutput, calls=%fused_computation.1 | convolution fusion | flops 4302307328 | bytes 13641728 | tf_op jit(solution)/shard_map/dot_general | solution.py:77
  46.7 104.8 %all_to_all.29 = bf16[32,64,2048]{2,1,0:T(8,128)(2,1)S(1)} all-to-all(bf16[32,64,2048]{2,1,0:T(8,128)(2,1)S(1)} %bitcast.38), channel_id=1, replica_groups=mesh['sp'=32,'tp'=4] {'sp'}, dimensions={0} | all-to-all | bytes 16777216 | tf_op jit(solution)/shard_map/all_to_all | solution.py:79
  151.5 4.5 %fusion.12 = f32[2048,512]{1,0:T(8,128)S(1)} fusion(bf16[2048,2048]{1,0:T(8,128)(2,1)S(1)} %bitcast.39, bf16[1,2048,512]{2,1,0:T(8,128)(2,1)S(1)} %copy-done.9), kind=kOutput, calls=%fused_computation.24 | convolution fusion | flops 4294967296 | bytes 14680064 | tf_op jit(solution)/shard_map/dot_general | solution.py:80
  156.1 5.2 %multiply_convert_fusion = bf16[2048,512]{1,0:T(8,128)(2,1)S(1)} fusion(f32[2048,512]{1,0:T(8,128)S(1)} %fusion.12, bf16[2048,2048]{1,0:T(8,128)(2,1)S(1)} %bitcast.40, bf16[1,2048,512]{2,1,0:T(8,128)(2,1)S(1)} %copy-done.10), kind=kOutput, calls=%fused_computation.5 | convolution fusion | flops 4301258752 | bytes 16777216 | tf_op jit(solution)/shard_map/dot_general | solution.py:81
  161.2 6.7 %convolution_convert_fusion = bf16[2048,2048]{1,0:T(8,128)(2,1)} fusion(bf16[2048,512]{1,0:T(8,128)(2,1)S(1)} %multiply_convert_fusion, bf16[1,512,2048]{2,1,0:T(8,128)(2,1)S(1)} %copy-done), kind=kOutput, calls=%fused_computation | convolution fusion | flops 4299161600 | bytes 12582912 | tf_op jit(solution)/shard_map/dot_general | solution.py:83
  168.0 5.1 %all-to-all-start.2 = ((bf16[32,64,2048]{2,1,0:T(8,128)(2,1)}), bf16[32,64,2048]{2,1,0:T(8,128)(2,1)}, u32[]{:S(2)}, u32[]{:S(2)}) async-start(bf16[32,64,2048]{2,1,0:T(8,128)(2,1)} %bitcast.37), calls=%async_computation.2 | async-start | bytes 16777216 | tf_op jit(solution)/shard_map/all_to_all | solution.py:85
  173.1 105.8 %all-to-all-done.2 = bf16[32,64,2048]{2,1,0:T(8,128)(2,1)} async-done(((bf16[32,64,2048]{2,1,0:T(8,128)(2,1)}), bf16[32,64,2048]{2,1,0:T(8,128)(2,1)}, u32[]{:S(2)}, u32[]{:S(2)}) %all-to-all-start.2) | async-done | bytes 8388640 | tf_op jit(solution)/shard_map/all_to_all | solution.py:85
  279.0 9.9 %fusion = bf16[512,2048]{1,0:T(8,128)(2,1)} fusion(f32[512,2048]{1,0:T(8,128)} %copy-done.1, bf16[32,64,2048]{2,1,0:T(8,128)(2,1)} %all-to-all-done.2, bf16[32,512]{1,0:T(8,128)(2,1)S(1)} %select_add_fusion, f32[32,512]{1,0:T(8,128)S(1)} %convolution_select_fusion, f32[64]{0:T(128)S(1)} %iota_convert_fusion), kind=kOutput, calls=%fused_computation.3 | convolution fusion | flops 4299161600 | bytes 14778624 | tf_op jit(solution)/shard_map/dot_general | solution.py:86
  (35 shorter events, 0.2 us)
Async XLA Ops:
  0.0 161.2 %copy-start = (bf16[1,512,2048]{2,1,0:T(8,128)(2,1)S(1)}, bf16[1,512,2048]{2,1,0:T(8,128)(2,1)}, u32[]{:S(2)}) copy-start(bf16[1,512,2048]{2,1,0:T(8,128)(2,1)} %param.25) | copy-start | bytes 6291460
  0.9 5.4 %copy-start.5 = (s32[2048]{0:T(1024)S(1)}, s32[2048]{0:T(1024)}, u32[]{:S(2)}) copy-start(s32[2048]{0:T(1024)} %param.18) | copy-start | bytes 24580
  1.7 4.5 %copy-start.6 = (bf16[3,256]{1,0:T(4,128)(2,1)S(1)}, bf16[3,256]{1,0:T(4,128)(2,1)}, u32[]{:S(2)}) copy-start(bf16[3,256]{1,0:T(4,128)(2,1)} %param.17) | copy-start | bytes 4612
  1.7 4.8 %copy-start.4 = (bf16[2048,256]{1,0:T(8,128)(2,1)S(1)}, bf16[2048,256]{1,0:T(8,128)(2,1)}, u32[]{:S(2)}) copy-start(bf16[2048,256]{1,0:T(8,128)(2,1)} %param.16) | copy-start | bytes 3145732
  1.7 4.6 %collective-permute-start = (f32[2,384]{1,0:T(2,128)S(1)}, f32[2,384]{1,0:T(2,128)S(1)}, u32[]{:S(2)}, u32[]{:S(2)}) collective-permute-start(f32[2,384]{1,0:T(2,128)S(1)} %pad_maximum_fusion.2), channel_id=1, source_target_pairs={{0,4},{4,8},{8,12},{12,16},{16,20},{20,24},{24,28},{28,32},{32,36}... | collective-permute-start | bytes 9224 | tf_op jit(solution)/shard_map/ppermute | solution.py:16
  12.4 5.1 %copy-start.7 = (s32[512,2]{0,1:T(2,128)S(1)}, s32[512,2]{0,1:T(2,128)}, u32[]{:S(2)}) copy-start(s32[512,2]{0,1:T(2,128)} %param.21) | copy-start | bytes 12292
  12.4 20.9 %all-to-all-start = ((bf16[4,512,256]{2,1,0:T(8,128)(2,1)}), bf16[4,512,256]{2,1,0:T(8,128)(2,1)S(1)}, u32[]{:S(2)}, u32[]{:S(2)}) async-start(bf16[4,512,256]{2,1,0:T(8,128)(2,1)} %bitcast.43), calls=%async_computation | async-start | bytes 2097152 | tf_op jit(solution)/shard_map/all_to_all | solution.py:53
  33.3 1.0 copy-start.2
  35.8 5.8 %copy-start.3 = (pred[2048,512]{1,0:T(32,128)(4,1)S(1)}, pred[2048,512]{1,0:T(32,128)(4,1)}, u32[]{:S(2)}) copy-start(pred[2048,512]{1,0:T(32,128)(4,1)} %bitcast_compare_fusion) | copy-start | bytes 3145732
  35.8 5.8 %copy-start.11 = (f32[2048]{0:T(1024)S(1)}, f32[2048]{0:T(1024)}, u32[]{:S(2)}) copy-start(f32[2048]{0:T(1024)} %param.20) | copy-start | bytes 24580
  41.6 5.1 %copy-start.1 = (f32[512,2048]{1,0:T(8,128)}, f32[512,2048]{1,0:T(8,128)S(1)}, u32[]{:S(2)}) copy-start(f32[512,2048]{1,0:T(8,128)S(1)} %get-tuple-element.15) | copy-start | bytes 12582916
  46.7 104.8 %copy-start.9 = (bf16[1,2048,512]{2,1,0:T(8,128)(2,1)S(1)}, bf16[1,2048,512]{2,1,0:T(8,128)(2,1)}, u32[]{:S(2)}) copy-start(bf16[1,2048,512]{2,1,0:T(8,128)(2,1)} %param.23) | copy-start | bytes 6291460
  151.5 4.5 %copy-start.10 = (bf16[1,2048,512]{2,1,0:T(8,128)(2,1)S(1)}, bf16[1,2048,512]{2,1,0:T(8,128)(2,1)}, u32[]{:S(2)}) copy-start(bf16[1,2048,512]{2,1,0:T(8,128)(2,1)} %param.24) | copy-start | bytes 6291460
  168.0 5.1 %copy-start.8 = (f32[512,2]{0,1:T(2,128)S(1)}, f32[512,2]{0,1:T(2,128)}, u32[]{:S(2)}) copy-start(f32[512,2]{0,1:T(2,128)} %param.22) | copy-start | bytes 12292
  168.0 111.0 %all-to-all-start.2 = ((bf16[32,64,2048]{2,1,0:T(8,128)(2,1)}), bf16[32,64,2048]{2,1,0:T(8,128)(2,1)}, u32[]{:S(2)}, u32[]{:S(2)}) async-start(bf16[32,64,2048]{2,1,0:T(8,128)(2,1)} %bitcast.37), calls=%async_computation.2 | async-start | bytes 16777216 | tf_op jit(solution)/shard_map/all_to_all | solution.py:85

commit v2 on v1

v2 whole, which is shorter than its diff:
```python
import jax
import jax.numpy as jnp
from jax import lax
from jax.experimental import pallas as pl
from jax.experimental.pallas import tpu as pltpu
from jax.sharding import PartitionSpec as P

EXPERTS = 32
CAP = 64
epsilon = 1e-06
F32 = jnp.float32
BF16 = jnp.bfloat16
MESH = pl.DeviceIdType.MESH
HALF = 256


def from_behind(x, axis, by):
    devices = lax.axis_size(axis)
    pairs = [(i, i + by) for i in range(devices) if 0 <= i + by < devices]
    return lax.ppermute(x, axis, pairs)


class Copies:
    def __init__(self, send_sem, recv_sem):
        self.send_sem, self.recv_sem = send_sem, recv_sem
        self.made = {}
        self.unsent = []

    def start(self, name, src, dst, device):
        i = len(self.made)
        copy = pltpu.make_async_remote_copy(
            src_ref=src,
            dst_ref=dst,
            send_sem=self.send_sem.at[i],
            recv_sem=self.recv_sem.at[i],
            device_id=device,
            device_id_type=MESH,
        )
        self.made[name] = copy
        self.unsent.append(name)
        copy.start()

    def arrived(self, name):
        self.made[name].wait_recv()

    def sent(self, name):
        self.made[name].wait_send()
        self.unsent.remove(name)

    def finish(self):
        for name in list(self.unsent):
            self.sent(name)


COPIES = 64
LOCALS = 16


def layer_kernel(
    gated,
    residual,
    proj,
    gain,
    table,
    w_gate,
    w_up,
    w_down,
    out,
    all_gate,
    all_up,
    all_down,
    a2a,
    res_v,
    proj_v,
    gain_v,
    hidden,
    tok,
    tables,
    dispatch,
    combine,
    rows_x,
    rows_di,
    rows_in,
    act,
    outs,
    outs_far,
    returned,
    land,
    buf_gate,
    buf_up,
    buf_down,
    send_sem,
    recv_sem,
    local_sem,
):
    sp, tp = lax.axis_index("sp"), lax.axis_index("tp")
    z, y, c = sp // 8, (sp // 2) % 4, sp % 2
    width = tok.shape[2]
    rows = tok.shape[1]

    def place(yy, zz, cc):
        return zz * 8 + yy * 2 + cc

    y_in, z_in = y + 1 - 2 * (y % 2), z + 1 - 2 * (z % 2)
    near_y, near_z = (place(y_in, z, c), tp), (place(y, z_in, c), tp)
    far_y, far_z = (place(3 - y, z, c), tp), (place(y, 3 - z, c), tp)
    far_d = (place(3 - y, 3 - z, c), tp)
    other = (place(y, z, 1 - c), tp)
    right, left = (sp, (tp + 1) % 4), (sp, (tp + 3) % 4)
    across = (sp, (tp + 2) % 4)
    chips = [(y, z), (y_in, z), (y, z_in), (y_in, z_in)]
    expert_of = [place(yy, zz, cc) for yy, zz in chips for cc in (c, 1 - c)]

    barrier = pltpu.get_barrier_semaphore()
    partners = [near_y, near_z, far_y, far_z, far_d, other, right, left, across]
    for partner in partners:
        pl.semaphore_signal(barrier, inc=1, device_id=partner, device_id_type=MESH)
    pl.semaphore_wait(barrier, len(partners))

    cp = Copies(send_sem, recv_sem)
    fetches = {}

    def fetch(name, i, src, dst):
        fetches[name] = pltpu.make_async_copy(src, dst, local_sem.at[i])
        fetches[name].start()

    def strip(k):
        return pl.ds(pl.multiple_of(k * rows, rows), rows)

    for name, dev in (("r", right), ("l", left), ("a", across)):
        cp.start("mix_" + name, gated.at[strip(dev[1])], a2a.at[tp], dev)
    fetch("mix", 0, gated.at[strip(tp)], a2a.at[tp])
    fetch("proj", 1, proj, proj_v)
    fetch("res", 2, residual, res_v)
    fetch("gain", 3, gain, gain_v)
    fetch("table", 4, table, tables.at[0])
    mine = strip(tp)
    for name, dev, slot in (("y", near_y, 1), ("z", near_z, 3)):
        cp.start("gate_" + name, w_gate.at[mine], all_gate.at[slot, mine], dev)
    for name, dev, slot in (("y", near_y, 1), ("z", near_z, 3)):
        cp.start("up_" + name, w_up.at[mine], all_up.at[slot, mine], dev)
    for name, dev, slot in (("y", near_y, 1), ("z", near_z, 3)):
        cp.start("down_" + name, w_down, all_down.at[slot], dev)
    for name, dev, slot in (("y", far_y, 1), ("z", far_z, 2), ("d", far_d, 3)):
        cp.start("table_" + name, table, tables.at[slot], dev)
    cp.start("own_gate", w_gate, all_gate.at[0], other)
    cp.start("own_up", w_up, all_up.at[0], other)
    cp.start("own_down", w_down, all_down.at[0], other)

    for name in ("mix", "proj", "res", "gain"):
        fetches[name].wait()
    for name in ("r", "l", "a"):
        cp.arrived("mix_" + name)
    step = 512
    squares = jnp.zeros((rows, 1), F32)
    for n in range(0, width, step):
        part = res_v[:, n : n + step].astype(F32)
        for j in range(4):
            part = part + jnp.dot(a2a[j], proj_v[j * 256 : (j + 1) * 256, n : n + step], preferred_element_type=F32)
        hidden[:, n : n + step] = part
        squares = squares + jnp.sum(part * part, axis=1, keepdims=True)
    scale = lax.rsqrt(squares * (1.0 / width) + epsilon)
    for n in range(0, width, step):
        tok[0, :, n : n + step] = (hidden[:, n : n + step] * scale * gain_v[:, n : n + step]).astype(BF16)
    cp.start("tok_y", tok.at[0], tok.at[1], far_y)
    cp.start("tok_z", tok.at[0], tok.at[2], far_z)

    for kind, store in (("gate", all_gate), ("up", all_up)):
        for name, slot in (("y", 1), ("z", 3)):
            cp.arrived(kind + "_" + name)
            cp.start(kind + "_r_" + name, store.at[slot, mine], store.at[slot, mine], right)
            cp.start(kind + "_l_" + name, store.at[slot, mine], store.at[slot, mine], left)

    fetches["table"].wait()

    def matches(source, pair):
        slot = lax.broadcasted_iota(jnp.int32, (CAP, rows), 0).astype(F32)
        halves, weights = [], []
        for k in range(2):
            e = expert_of[2 * pair + k]
            hit = tables[source, pl.ds(e, 1), :] == slot
            halves.append(jnp.where(hit, 1.0, 0.0))
            weights.append(jnp.where(hit, tables[source, pl.ds(EXPERTS + e, 1), :], 0.0))
        return jnp.concatenate(halves, axis=0), jnp.concatenate(weights, axis=0)

    def gather(source, place_in, far):
        for pair in range(4):
            dispatch[pair * 128 : (pair + 1) * 128, :] = matches(source, pair)[0].astype(BF16)
        for n in range(0, width, step):
            got = jnp.dot(dispatch[...], tok[source, :, n : n + step], preferred_element_type=F32).astype(BF16)
            for e in range(6):
                rows_x[e, place_in * CAP : (place_in + 1) * CAP, n : n + step] = got[e * CAP : (e + 1) * CAP]
            rows_di[far, :, n : n + step] = got[6 * CAP :]

    def scatter(source, place_in, far, store):
        for pair in range(4):
            combine[:, pair * 128 : (pair + 1) * 128] = matches(source, pair)[1].T.astype(BF16)
        for n in range(0, width, step):
            total = jnp.dot(combine[:, :384], outs[place_in, :, n : n + step], preferred_element_type=F32)
            total = total + jnp.dot(combine[:, 384:], returned[far, :, n : n + step], preferred_element_type=F32)
            store(n, total)

    def load(e, slot):
        gate_from = w_gate if e == 0 else all_gate.at[e - 1]
        up_from = w_up if e == 0 else all_up.at[e - 1]
        down_from = w_down if e == 0 else all_down.at[e - 1]
        fetch(f"g{slot}", 5 + slot * 3, gate_from, buf_gate.at[slot])
        fetch(f"u{slot}", 6 + slot * 3, up_from, buf_up.at[slot])
        fetch(f"d{slot}", 7 + slot * 3, down_from, buf_down.at[slot])

    def feed_forward(e, slot, far):
        high = 128 if e < 2 else 192
        if e >= 2:
            far_in = far + 1 if e < 4 else far
            rows_x[e, 128:192, :] = rows_in[far_in, (e % 2) * CAP : (e % 2 + 1) * CAP, :]
        fetches[f"g{slot}"].wait()
        fetches[f"u{slot}"].wait()
        for n in range(0, 512, 256):
            left_side = rows_x[e, :high, :]
            gate_val = jnp.dot(left_side, buf_gate[slot, :, n : n + 256], preferred_element_type=F32)
            up_val = jnp.dot(left_side, buf_up[slot, :, n : n + 256], preferred_element_type=F32)
            act[:high, n : n + 256] = (gate_val / (1.0 + jnp.exp(-gate_val)) * up_val).astype(BF16)
        fetches[f"d{slot}"].wait()
        for n in range(0, width, step):
            got = jnp.dot(act[:high, :], buf_down[slot, :, n : n + step], preferred_element_type=F32).astype(BF16)
            for k in range(2):
                outs[k, e * CAP : (e + 1) * CAP, n : n + step] = got[k * CAP : (k + 1) * CAP]
            if e >= 2:
                far_in = far + 1 if e < 4 else far
                outs_far[far_in, (e % 2) * CAP : (e % 2 + 1) * CAP, n : n + step] = got[128:192]

    def ask(batch, k):
        dev = near_y if k == 0 else near_z
        cp.start(f"ask{batch}{k}", rows_di.at[2 * batch + k], rows_in.at[2 * batch + k], dev)

    def answer(batch, k):
        dev = near_y if k == 0 else near_z
        cp.start(f"ans{batch}{k}", outs_far.at[2 * batch + k], returned.at[2 * batch + k], dev)

    before, after = strip((tp + 3) % 4), strip((tp + 1) % 4)
    for name, slot in (("y", 1), ("z", 3)):
        cp.arrived("gate_r_" + name)
        cp.start("gate_f_" + name, all_gate.at[slot, before], all_gate.at[slot, before], right)
    for name, slot in (("y", 1), ("z", 3)):
        cp.arrived("up_l_" + name)
        cp.start("up_f_" + name, all_up.at[slot, after], all_up.at[slot, after], left)

    cp.arrived("tok_y")
    cp.arrived("tok_z")
    cp.start("tok_fy", tok.at[1, :HALF], tok.at[3, :HALF], far_z)
    cp.start("tok_fz", tok.at[2, HALF:], tok.at[3, HALF:], far_y)
    for name in ("y", "z", "d"):
        cp.arrived("table_" + name)

    gather(1, 0, 0)
    ask(0, 0)
    gather(2, 1, 1)
    ask(0, 1)
    for name in ("gate", "up", "down"):
        cp.arrived("own_" + name)
    load(0, 0)
    load(1, 1)
    feed_forward(0, 0, 0)
    for name, slot in (("y", 1), ("z", 3)):
        cp.arrived("down_" + name)
        cp.start("down_o_" + name, all_down.at[slot], all_down.at[slot + 1], other)
        cp.arrived("gate_l_" + name)
        cp.arrived("gate_f_" + name)
        cp.start("gate_o_" + name, all_gate.at[slot], all_gate.at[slot + 1], other)
        cp.arrived("up_r_" + name)
        cp.arrived("up_f_" + name)
        cp.start("up_o_" + name, all_up.at[slot], all_up.at[slot + 1], other)
    load(2, 0)
    feed_forward(1, 1, 0)
    cp.arrived("down_o_y")
    cp.arrived("gate_o_y")
    cp.arrived("up_o_y")
    load(3, 1)
    cp.arrived("ask01")
    feed_forward(2, 0, 0)
    load(4, 0)
    feed_forward(3, 1, 0)
    answer(0, 1)
    cp.arrived("down_o_z")
    cp.arrived("gate_o_z")
    cp.arrived("up_o_z")
    load(5, 1)
    cp.arrived("ask00")
    feed_forward(4, 0, 0)
    feed_forward(5, 1, 0)
    answer(0, 0)
    load(0, 0)
    load(1, 1)
    cp.arrived("tok_fy")
    cp.arrived("tok_fz")
    gather(0, 0, 2)
    ask(1, 0)
    gather(3, 1, 3)
    ask(1, 1)

    def into(k):
        def store(n, total):
            tok[k, :, n : n + step] = total.astype(BF16)

        return store

    cp.arrived("ans00")
    cp.sent("tok_fy")
    scatter(1, 0, 0, into(1))
    cp.start("pure_y", tok.at[1, :HALF], land.at[0], far_y)
    cp.arrived("ans01")
    cp.sent("tok_fz")
    scatter(2, 1, 1, into(2))
    cp.start("pure_z", tok.at[2, HALF:], land.at[1], far_z)

    feed_forward(0, 0, 2)
    load(2, 0)
    feed_forward(1, 1, 2)
    load(3, 1)
    cp.arrived("ask11")
    feed_forward(2, 0, 2)
    load(4, 0)
    feed_forward(3, 1, 2)
    answer(1, 1)
    load(5, 1)
    cp.arrived("ask10")
    feed_forward(4, 0, 2)
    feed_forward(5, 1, 2)
    answer(1, 0)
    cp.arrived("ans11")
    scatter(3, 1, 3, into(3))
    cp.start("diag_y", tok.at[3, :HALF], land.at[2], far_y)
    cp.start("diag_z", tok.at[3, HALF:], land.at[3], far_z)

    def onto_hidden(n, total):
        hidden[:, n : n + step] = hidden[:, n : n + step] + total

    cp.arrived("ans10")
    scatter(0, 0, 2, onto_hidden)

    cp.arrived("diag_y")
    tok[2, :HALF, :] = (tok[2, :HALF, :].astype(F32) + land[2].astype(F32)).astype(BF16)
    cp.start("fwd_z", tok.at[2, :HALF], land.at[4], far_z)
    cp.arrived("diag_z")
    tok[1, HALF:, :] = (tok[1, HALF:, :].astype(F32) + land[3].astype(F32)).astype(BF16)
    cp.start("fwd_y", tok.at[1, HALF:], land.at[5], far_y)
    cp.arrived("pure_y")
    hidden[:HALF, :] = hidden[:HALF, :] + land[0].astype(F32)
    cp.arrived("pure_z")
    hidden[HALF:, :] = hidden[HALF:, :] + land[1].astype(F32)
    cp.arrived("fwd_z")
    out[:HALF, :] = (hidden[:HALF, :] + land[4].astype(F32)).astype(BF16)
    cp.arrived("fwd_y")
    out[HALF:, :] = (hidden[HALF:, :] + land[5].astype(F32)).astype(BF16)
    cp.finish()


def layer(gated, residual, proj, gain, table, w_gate, w_up, w_down):
    rows, width = residual.shape
    hid = w_gate.shape[1]
    any_spec = pl.BlockSpec(memory_space=pl.ANY)
    shapes = (
        jax.ShapeDtypeStruct((rows, width), BF16),
        jax.ShapeDtypeStruct((5, width, hid), BF16),
        jax.ShapeDtypeStruct((5, width, hid), BF16),
        jax.ShapeDtypeStruct((5, hid, width), BF16),
    )
    return pl.pallas_call(
        layer_kernel,
        out_shape=shapes,
        in_specs=[any_spec] * 8,
        out_specs=(pl.BlockSpec(memory_space=pltpu.VMEM), any_spec, any_spec, any_spec),
        scratch_shapes=[
            pltpu.VMEM((4, rows, 256), BF16),
            pltpu.VMEM((rows, width), BF16),
            pltpu.VMEM((1024, width), BF16),
            pltpu.VMEM((1, width), F32),
            pltpu.VMEM((rows, width), F32),
            pltpu.VMEM((4, rows, width), BF16),
            pltpu.VMEM((4, 2 * EXPERTS, rows), F32),
            pltpu.VMEM((512, rows), BF16),
            pltpu.VMEM((rows, 512), BF16),
            pltpu.VMEM((6, 192, width), BF16),
            pltpu.VMEM((4, 128, width), BF16),
            pltpu.VMEM((4, 128, width), BF16),
            pltpu.VMEM((192, hid), BF16),
            pltpu.VMEM((2, 384, width), BF16),
            pltpu.VMEM((4, 128, width), BF16),
            pltpu.VMEM((4, 128, width), BF16),
            pltpu.VMEM((6, HALF, width), BF16),
            pltpu.VMEM((2, width, hid), BF16),
            pltpu.VMEM((2, width, hid), BF16),
            pltpu.VMEM((2, hid, width), BF16),
            pltpu.SemaphoreType.DMA((COPIES,)),
            pltpu.SemaphoreType.DMA((COPIES,)),
            pltpu.SemaphoreType.DMA((LOCALS,)),
        ],
        compiler_params=pltpu.CompilerParams(
            collective_id=0, has_side_effects=True, vmem_limit_bytes=67043328
        ),
        name="layer",
    )(gated, residual, proj, gain, table, w_gate, w_up, w_down)[0]


def per_device(
    residual_in,
    conv_input,
    input_gate,
    output_gate,
    conv_taps,
    doc_ids,
    proj_weight,
    norm_gain,
    expert_ids,
    expert_weight,
    w_gate,
    w_up,
    w_down,
):
    kernel_width = conv_taps.shape[0]
    rim = kernel_width - 1
    length, channels = conv_input.shape
    doc_float = doc_ids.astype(F32)
    tail = input_gate[-rim:].astype(F32) * conv_input[-rim:].astype(F32)
    packed = jnp.concatenate([tail, jnp.broadcast_to(doc_float[-rim:, None], (rim, 128))], axis=1)
    prev = from_behind(packed, "sp", 1)
    prev_in, prev_ids = prev[:, :channels], prev[:, channels]
    product = input_gate.astype(F32) * conv_input.astype(F32)
    padded_in = jnp.concatenate([prev_in, product], axis=0)
    padded_ids = jnp.concatenate([prev_ids, doc_float], axis=0)
    conv_sum = jnp.zeros(product.shape, F32)
    for offset in range(kernel_width):
        same_doc = padded_ids[offset : offset + length] == doc_float
        term = conv_taps[offset].astype(F32)[None, :] * padded_in[offset : offset + length]
        conv_sum = conv_sum + jnp.where(same_doc[:, None], term, 0.0)
    gated = (output_gate.astype(F32) * conv_sum).astype(BF16)

    tokens = expert_ids.shape[0]
    experts = jnp.arange(EXPERTS, dtype=jnp.int32)
    ids_t = expert_ids.T
    weight_t = expert_weight.T
    hit = [ids_t[j][None, :] == experts[:, None] for j in range(2)]
    used = hit[0] | hit[1]
    weight_of = jnp.where(hit[0], weight_t[0][None, :], 0.0) + jnp.where(hit[1], weight_t[1][None, :], 0.0)
    t_row = lax.broadcasted_iota(jnp.int32, (tokens, tokens), 0)
    t_col = lax.broadcasted_iota(jnp.int32, (tokens, tokens), 1)
    earlier = (t_row < t_col).astype(BF16)
    rank = jnp.dot(used.astype(BF16), earlier, preferred_element_type=F32)
    code = jnp.where(used, rank, -1.0)
    table = jnp.concatenate([code, weight_of], axis=0)
    return layer(
        gated, residual_in, proj_weight, norm_gain[None, :], table, w_gate[0], w_up[0], w_down[0]
    )


def solution(mesh):
    return jax.shard_map(
        per_device,
        mesh=mesh,
        in_specs=(
            P(("sp", "tp"), None),
            P("sp", "tp"),
            P("sp", "tp"),
            P("sp", "tp"),
            P(None, "tp"),
            P("sp"),
            P(),
            P(),
            P(("sp", "tp"), None),
            P(("sp", "tp"), None),
            P("sp", None, None),
            P("sp", None, None),
            P("sp", None, None),
        ),
        out_specs=P(("sp", "tp"), None),
        check_vma=False,
    )
```

time: 289 us -> 212 us (0.73)
  Pallas kernels: 0 us -> 198 us
  waiting for transfers between devices: 120 us -> 0.01 us
  blocking collectives: 105 us -> 0 us
  matrix products: 37.4 us -> 0.19 us
  starting transfers between devices: 11.5 us -> 1.28 us
  other arithmetic: 12.4 us -> 8.09 us
    pallas_call x0 -> x1, Pallas kernels: none -> 198 us  [layer(): pl.pallas_call(layer_kernel, out_shape=shapes, in_specs=[any_spec] * 8, o...]
    all_to_all x2 -> x0, waiting for transfers between devices: 120 us -> none  [the longest x1 106 us: per_device(): lax.all_to_all(expert_out, 'sp', split_axis=0, concat_axis=0, tiled=True)]
    all_to_all x1 -> x0, blocking collectives: 105 us -> none  [per_device(): lax.all_to_all(buffer, 'sp', split_axis=0, concat_axis=0, tiled=True)]
    dot_general x6 -> x0, matrix products: 37.2 us -> none  [the longest x1 9.88 us: per_device(): lax.dot_general(combine, returned, (((0,), (0,)), ((), ())), preferred_el...]
    all_to_all x2 -> x0, starting transfers between devices: 10.1 us -> none  [the longest x1 5.09 us: per_device(): lax.all_to_all(expert_out, 'sp', split_axis=0, concat_axis=0, tiled=True)]
  transfers between devices with their start and end apart: 3 -> 1, of which waited for: 2 -> 0; matrix products, arithmetic and copies ran while one was open for 2% -> 2% of each run, Pallas kernels for 0% -> 0%
where the time goes in v2:
time: 212 us; the launch traced here: 211 us
  Pallas kernels  198 us (93%)
  other arithmetic  8.09 us (4%)
  local copies, waits for them, and re-layouts  3.45 us (2%)
    pallas_call x1, Pallas kernels, layer(): pl.pallas_call(layer_kernel, out_shape=shapes, in_specs=[any_spec] * 8, o...  198 us
  transfers between devices with their start and end apart: 1, of which 0 were waited for; matrix products, arithmetic and copies ran while one was open for 2% of the time, Pallas kernels for 0%

profile of v2, /device:TPU:0, one launch (start us, length us, event | category | flops | bytes accessed | tf_op | source)
XLA Modules:
  0.0 211.3 jit_solution(2276445138424159875)
XLA Ops:
  0.0 0.7 convert_element_type.32
  0.7 0.1 slice.64
  0.8 0.7 convert_multiply_fusion.1
  1.5 0.1 broadcast_in_dim.67
  1.6 1.3 collective-permute-start
  2.8 0.7 convert_compare_fusion
  3.6 0.0 copy-start.1
  3.6 0.0 copy-start.2
  3.6 0.0 copy-start.3
  3.6 0.0 copy-start
  3.6 1.9 convert_multiply_fusion
  5.4 0.0 copy-done.1
  5.5 0.0 copy-done.2
  5.5 0.0 copy-done.3
  5.5 0.2 convolution_select_fusion
  5.7 0.7 pad_maximum_fusion.1.table
  6.4 0.0 collective-permute-done
  6.4 0.1 slice_reduce_fusion
  6.5 0.1 fusion.14
  6.6 0.0 copy-done
  6.6 3.4 %fusion.6.gated = bf16[2048,256]{1,0:T(8,128)(2,1)} fusion(f32[2,256]{1,0:T(2,128)S(1)} %slice.68, f32[2048,256]{1,0:T(8,128)S(1)} %convert_multiply_fusion, bf16[2048,256]{1,0:T(8,128)(2,1)S(1)} %copy-done, f32[256]{0:T(256)S(1)} %bitcast.24, f32[256]{0:T(256)S(1)} %bitcast.25, f32[256]{0:T(256)S(1)} %bitcast.23, ...), kind=kLoop, calls=%fused_computation.8 | loop fusion | flops 6815744 | bytes 4205568 | tf_op jit(solution)/shard_map/convert_element_type | solution.py:436
  9.9 198.2 %layer.1 = (bf16[512,2048]{1,0:T(8,128)(2,1)}, bf16[5,2048,512]{2,1,0:T(8,128)(2,1)}, bf16[5,2048,512]{2,1,0:T(8,128)(2,1)}, bf16[5,512,2048]{2,1,0:T(8,128)(2,1)}) custom-call(bf16[2048,256]{1,0:T(8,128)(2,1)} %fusion.6.gated, bf16[512,2048]{1,0:T(8,128)(2,1)} %residual.1, bf16[1024,2048]{1,0:T(8,128)(2,1)} %proj.1, f32[1,2048]{1,0:T(1,128)} %bitcast.16, ...), custom_call_target="tpu_custom_call" | custom-call | tf_op jit(solution)/shard_map/layer/pallas_call | solution.py:368
  208.2 3.2 %copy.15 = bf16[512,2048]{1,0:T(8,128)(2,1)} copy(bf16[512,2048]{1,0:T(8,128)(2,1)} %get-tuple-element.6) | data formatting | bytes 4194304
  (6 shorter events, 0.0 us)
Async XLA Ops:
  1.6 4.8 %collective-permute-start = (f32[2,384]{1,0:T(2,128)S(1)}, f32[2,384]{1,0:T(2,128)S(1)}, u32[]{:S(2)}, u32[]{:S(2)}) collective-permute-start(f32[2,384]{1,0:T(2,128)S(1)} %pad_maximum_fusion.3), channel_id=1, source_target_pairs={{0,4},{4,8},{8,12},{12,16},{16,20},{20,24},{24,28},{28,32},{32,36}... | collective-permute-start | bytes 9224 | tf_op jit(solution)/shard_map/ppermute | solution.py:20
  3.6 1.9 copy-start.1
  3.6 1.9 copy-start.2
  3.6 1.9 copy-start.3
  3.6 3.0 %copy-start = (bf16[2048,256]{1,0:T(8,128)(2,1)S(1)}, bf16[2048,256]{1,0:T(8,128)(2,1)}, u32[]{:S(2)}) copy-start(bf16[2048,256]{1,0:T(8,128)(2,1)} %param.16) | copy-start | bytes 3145732

commit v3 on v0

v3 whole, which is shorter than its diff:
```python
import jax
import jax.numpy as jnp
from jax import lax
from jax.experimental import pallas as pl
from jax.experimental.pallas import tpu as pltpu
from jax.sharding import PartitionSpec as P

EXPERTS = 32
CAP = 64
epsilon = 1e-06
F32 = jnp.float32
BF16 = jnp.bfloat16
MESH = pl.DeviceIdType.MESH
HALF = 256
DIRECT = 128


class Copies:
    def __init__(self, send_sem, recv_sem):
        self.send_sem, self.recv_sem = send_sem, recv_sem
        self.made = {}
        self.unsent = []

    def start(self, name, src, dst, device):
        i = len(self.made)
        copy = pltpu.make_async_remote_copy(
            src_ref=src,
            dst_ref=dst,
            send_sem=self.send_sem.at[i],
            recv_sem=self.recv_sem.at[i],
            device_id=device,
            device_id_type=MESH,
        )
        self.made[name] = copy
        self.unsent.append(name)
        copy.start()

    def arrived(self, name):
        self.made[name].wait_recv()

    def sent(self, name):
        self.made[name].wait_send()
        self.unsent.remove(name)

    def finish(self):
        for name in list(self.unsent):
            self.sent(name)


COPIES = 96
LOCALS = 24
A_COLS, B_COLS = slice(0, 1024), slice(1024, 2048)


def layer_kernel(
    residual,
    conv_input,
    input_gate,
    output_gate,
    taps,
    docs,
    proj,
    gain,
    ids,
    route_weight,
    w_gate,
    w_up,
    w_down,
    hidden_out,
    far_out,
    all_gate,
    all_up,
    all_down,
    taps_v,
    docs_v,
    ids_v,
    route_v,
    halo_c,
    halo_g,
    halo_d,
    product,
    doc_rows,
    gated,
    a2a,
    gain_v,
    hidden,
    tok,
    tables,
    dispatch,
    combine,
    rows_x,
    rows_di,
    rows_in,
    act,
    outs,
    outs_far,
    returned,
    land,
    buf_gate,
    buf_up,
    buf_down,
    send_sem,
    recv_sem,
    local_sem,
):
    sp, tp = lax.axis_index("sp"), lax.axis_index("tp")
    z, y, c = sp // 8, (sp // 2) % 4, sp % 2
    rows, width = tok.shape[1], tok.shape[2]
    length = gated.shape[0]

    def place(yy, zz, cc):
        return zz * 8 + yy * 2 + cc

    y_in, z_in = y + 1 - 2 * (y % 2), z + 1 - 2 * (z % 2)
    near_y, near_z = (place(y_in, z, c), tp), (place(y, z_in, c), tp)
    far_y, far_z = (place(3 - y, z, c), tp), (place(y, 3 - z, c), tp)
    far_d = (place(3 - y, 3 - z, c), tp)
    other = (place(y, z, 1 - c), tp)
    right, left = (sp, (tp + 1) % 4), (sp, (tp + 3) % 4)
    across = (sp, (tp + 2) % 4)
    ahead, behind = ((sp + 1) % 32, tp), ((sp + 31) % 32, tp)
    chips = [(y, z), (y_in, z), (y, z_in), (y_in, z_in)]
    expert_of = [place(yy, zz, cc) for yy, zz in chips for cc in (c, 1 - c)]

    barrier = pltpu.get_barrier_semaphore()
    partners = [near_y, near_z, far_y, far_z, far_d, other, right, left, across, ahead, behind]
    for partner in partners:
        pl.semaphore_signal(barrier, inc=1, device_id=partner, device_id_type=MESH)

    cp = Copies(send_sem, recv_sem)
    fetches = {}

    def fetch(name, src, dst, i=None):
        i = 9 + len(fetches) if i is None else i
        fetches[name] = pltpu.make_async_copy(src, dst, local_sem.at[i])
        fetches[name].start()

    def strip(k):
        return pl.ds(pl.multiple_of(k * rows, rows), rows)

    conv_v, in_gate_v = buf_gate.at[0, :, :256], buf_gate.at[0, :, 256:]
    out_gate_v = buf_gate.at[1, :, :256]
    fetch("conv", conv_input, conv_v)
    fetch("in_gate", input_gate, in_gate_v)
    fetch("out_gate", output_gate, out_gate_v)
    fetch("taps", taps, taps_v)
    fetch("docs", docs, docs_v)
    fetch("ids", ids, ids_v)
    fetch("route", route_weight, route_v)
    fetch("gain", gain, gain_v)
    fetch("proj0", proj.at[:512], buf_down.at[0])
    fetch("proj1", proj.at[512:], buf_down.at[1])
    fetch("res0", residual.at[:256], rows_x.at[0])
    fetch("res1", residual.at[256:], rows_x.at[1])
    pl.semaphore_wait(barrier, len(partners))

    cp.start("halo_c", conv_input.at[length - 16 :], halo_c, ahead)
    cp.start("halo_g", input_gate.at[length - 16 :], halo_g, ahead)
    cp.start("halo_d", docs.at[8:], halo_d, ahead)
    mine = strip(tp)
    near = (("y", near_y, 1), ("z", near_z, 3))
    for name, dev, slot in near:
        cp.start("gate_" + name, w_gate.at[mine], all_gate.at[slot, mine], dev)
    for name, dev, slot in near:
        cp.start("up_" + name, w_up.at[mine], all_up.at[slot, mine], dev)
    late = pl.ds(pl.multiple_of(((tp + 2) % 4) * rows + rows - DIRECT, DIRECT), DIRECT)
    cp.start("gate_d_y", w_gate.at[late], all_gate.at[1, late], near_y)
    cp.start("up_d_z", w_up.at[late], all_up.at[3, late], near_z)
    for name, dev, slot in near:
        cp.start("down_" + name, w_down, all_down.at[slot], dev)
    cp.start("own_gate", w_gate, all_gate.at[0], other)
    cp.start("own_up", w_up, all_up.at[0], other)
    cp.start("own_down", w_down, all_down.at[0], other)

    for name in ("conv", "in_gate", "out_gate", "taps", "docs"):
        fetches[name].wait()
    for r in range(length // 128):
        doc_rows[8 + r * 128 : 136 + r * 128, :] = jnp.broadcast_to(
            docs_v[r : r + 1, :].astype(F32), (128, 128)
        ).T
    for r in range(0, length, 256):
        product[8 + r : 264 + r, :] = buf_gate[0, r : r + 256, :256].astype(F32) * buf_gate[
            0, r : r + 256, 256:
        ].astype(F32)
    tap = [taps_v[k : k + 1, :].astype(F32) for k in range(3)]

    def convolve(r):
        here = doc_rows[8 + r : 264 + r, :]
        same = [doc_rows[6 + k + r : 262 + k + r, :] == here for k in range(2)]
        for h in (0, 128):
            total = tap[2][:, h : h + 128] * product[8 + r : 264 + r, h : h + 128]
            for k in range(2):
                term = tap[k][:, h : h + 128] * product[6 + k + r : 262 + k + r, h : h + 128]
                total = total + jnp.where(same[k], term, 0.0)
            gated[r : r + 256, h : h + 128] = (
                buf_gate[1, r : r + 256, h : h + 128].astype(F32) * total
            ).astype(BF16)

    for r in range(256, length, 256):
        convolve(r)
    cp.arrived("halo_c")
    cp.arrived("halo_g")
    cp.arrived("halo_d")
    product[:8, :] = (halo_c[...].astype(F32) * halo_g[...].astype(F32))[8:]
    halo_docs = jnp.broadcast_to(halo_d[7:8, :].astype(F32), (128, 128)).T
    doc_rows[:8, :] = jnp.where(sp == 0, -1.0, halo_docs[120:])
    convolve(0)

    for name, dev in (("r", right), ("l", left), ("a", across)):
        cp.start("mix_" + name, gated.at[strip(dev[1])], a2a.at[tp], dev)
    fetch("mix", gated.at[strip(tp)], a2a.at[tp])

    def share(kind, name, part, at):
        store = all_gate if kind == "gate" else all_up
        slot = 1 if name == "y" else 3
        cp.start(f"{kind}_o{part}_{name}", store.at[slot, at], store.at[slot + 1, at], other)

    def turn(kind, way, name, part, at):
        store = all_gate if kind == "gate" else all_up
        slot = 1 if name == "y" else 3
        cp.start(
            f"{kind}_{part}_{name}", store.at[slot, at], store.at[slot, at], right if way == "r" else left
        )

    before, after, opposite = strip((tp + 3) % 4), strip((tp + 1) % 4), strip((tp + 2) % 4)

    def early(k):
        return pl.ds(pl.multiple_of((k % 4) * rows, rows), rows - DIRECT)

    for name in ("y", "z"):
        cp.arrived("gate_" + name)
        turn("gate", "r", name, "r", mine)
        turn("gate", "l", name, "l", mine)
        share("gate", name, "m", mine)

    fetches["ids"].wait()
    fetches["route"].wait()
    experts = lax.broadcasted_iota(jnp.int32, (EXPERTS, rows), 0)
    hit = [ids_v[j : j + 1, :] == experts for j in range(2)]
    used = jnp.where(hit[0], 1.0, jnp.where(hit[1], 1.0, 0.0))
    earlier = lax.broadcasted_iota(jnp.int32, (rows, rows), 0) < lax.broadcasted_iota(jnp.int32, (rows, rows), 1)
    dispatch[...] = jnp.where(earlier, 1.0, 0.0).astype(BF16)
    rank = jnp.dot(used.astype(BF16), dispatch[...], preferred_element_type=F32)
    tables[0, :EXPERTS, :] = jnp.where(used > 0.0, rank, -1.0)
    tables[0, EXPERTS:, :] = jnp.where(hit[0], route_v[0:1, :], jnp.where(hit[1], route_v[1:2, :], 0.0))

    for name, dev, slot in (("y", far_y, 1), ("z", far_z, 2), ("d", far_d, 3)):
        cp.start("table_" + name, tables.at[0], tables.at[slot], dev)

    for name in ("mix", "proj0", "proj1", "res0", "res1", "gain"):
        fetches[name].wait()
    for name in ("r", "l", "a"):
        cp.arrived("mix_" + name)
    step = 512

    def project():
        squares = jnp.zeros((rows, 1), F32)
        for n in range(0, width, step):
            part = jnp.concatenate([rows_x[0, :, n : n + step], rows_x[1, :, n : n + step]], axis=0).astype(F32)
            for j in range(4):
                part = part + jnp.dot(
                    a2a[j],
                    buf_down[j // 2, (j % 2) * 256 : (j % 2 + 1) * 256, n : n + step],
                    preferred_element_type=F32,
                )
            hidden[:, n : n + step] = part
            squares = squares + jnp.sum(part * part, axis=1, keepdims=True)
        scale = lax.rsqrt(squares * (1.0 / width) + epsilon)
        for n in range(0, width, step):
            tok[0, :, n : n + step] = (hidden[:, n : n + step] * scale * gain_v[:, n : n + step]).astype(BF16)

    project()
    cp.start("tok_y", tok.at[0], tok.at[1], far_y)
    cp.start("tok_z", tok.at[0], tok.at[2], far_z)

    def matches(source, pair):
        slot = lax.broadcasted_iota(jnp.int32, (CAP, rows), 0).astype(F32)
        halves, weights = [], []
        for k in range(2):
            e = expert_of[2 * pair + k]
            same = tables[source, pl.ds(e, 1), :] == slot
            halves.append(jnp.where(same, 1.0, 0.0))
            weights.append(jnp.where(same, tables[source, pl.ds(EXPERTS + e, 1), :], 0.0))
        return jnp.concatenate(halves, axis=0), jnp.concatenate(weights, axis=0)

    source_of = [1, 2, 0, 3]

    def gather(i):
        source = source_of[i]
        for pair in range(4):
            dispatch[pair * 128 : (pair + 1) * 128, :] = matches(source, pair)[0].astype(BF16)
        for n in range(0, width, step):
            got = jnp.dot(dispatch[...], tok[source, :, n : n + step], preferred_element_type=F32).astype(BF16)
            for e in range(6):
                rows_x[e, i * CAP : (i + 1) * CAP, n : n + step] = got[e * CAP : (e + 1) * CAP]
            rows_di[i, :, n : n + step] = got[6 * CAP :]

    def weigh(i):
        for pair in range(4):
            combine[:, pair * 128 : (pair + 1) * 128] = matches(source_of[i], pair)[1].T.astype(BF16)

    def scatter(i, cols, store):
        for n in range(cols.start, cols.stop, step):
            total = jnp.dot(combine[:, :384], outs[i, :, n : n + step], preferred_element_type=F32)
            total = total + jnp.dot(combine[:, 384:], returned[i, :, n : n + step], preferred_element_type=F32)
            store(n, total)

    def load(e, slot):
        gate_from = w_gate if e == 0 else all_gate.at[e - 1]
        up_from = w_up if e == 0 else all_up.at[e - 1]
        down_from = w_down if e == 0 else all_down.at[e - 1]
        fetch(f"g{slot}", gate_from, buf_gate.at[slot], slot * 3)
        fetch(f"u{slot}", up_from, buf_up.at[slot], slot * 3 + 1)
        fetch(f"d{slot}", down_from, buf_down.at[slot], slot * 3 + 2)

    def loaded(slot):
        for kind in "gud":
            fetches[f"{kind}{slot}"].wait()

    def activate(slot, left_ref, high):
        for n in range(0, 512, 256):
            left_side = left_ref[...]
            gate_val = jnp.dot(left_side, buf_gate[slot, :, n : n + 256], preferred_element_type=F32)
            up_val = jnp.dot(left_side, buf_up[slot, :, n : n + 256], preferred_element_type=F32)
            act[:high, n : n + 256] = (gate_val / (1.0 + jnp.exp(-gate_val)) * up_val).astype(BF16)

    def local(e, slot, batch):
        activate(slot, rows_x.at[e, batch * 128 : (batch + 1) * 128], 128)
        for n in range(0, width, step):
            got = jnp.dot(act[...], buf_down[slot, :, n : n + step], preferred_element_type=F32).astype(BF16)
            for k in range(2):
                outs[2 * batch + k, e * CAP : (e + 1) * CAP, n : n + step] = got[k * CAP : (k + 1) * CAP]

    def distant(e, slot, i):
        at = slice((e % 2) * CAP, (e % 2 + 1) * CAP)
        activate(slot, rows_in.at[i, at], CAP)
        for n in range(0, width, step):
            outs_far[i, at, n : n + step] = jnp.dot(
                act[:CAP, :], buf_down[slot, :, n : n + step], preferred_element_type=F32
            ).astype(BF16)

    def ask(i):
        cp.start(f"ask{i}", rows_di.at[i], rows_in.at[i], near_y if i % 2 == 0 else near_z)

    def answer(e, i, order):
        at = slice((e % 2) * CAP, (e % 2 + 1) * CAP)
        for half in order:
            cols = A_COLS if half == "a" else B_COLS
            cp.start(
                f"ans{i}{e % 2}{half}",
                outs_far.at[i, at, cols],
                returned.at[i, at, cols],
                near_y if i % 2 == 0 else near_z,
            )

    def answered(i, half):
        for k in range(2):
            cp.arrived(f"ans{i}{k}{half}")

    gather(2)
    cp.arrived("up_y")
    turn("up", "r", "y", "r", mine)
    turn("up", "l", "y", "l", mine)
    share("up", "y", "m", mine)
    cp.arrived("gate_r_y")
    turn("gate", "r", "y", "f", early(tp + 3))
    share("gate", "y", "r", before)
    cp.arrived("up_z")
    turn("up", "r", "z", "r", mine)
    share("up", "z", "m", mine)
    cp.arrived("gate_l_y")
    share("gate", "y", "l", after)
    cp.arrived("gate_r_z")
    turn("gate", "r", "z", "f", before)
    share("gate", "z", "r", before)
    cp.arrived("up_d_z")
    share("up", "z", "d", late)
    cp.arrived("gate_l_z")
    share("gate", "z", "l", after)
    cp.arrived("up_l_y")
    turn("up", "l", "y", "f", after)
    turn("up", "l", "z", "l", mine)
    share("up", "y", "l", after)
    cp.arrived("up_r_y")
    share("up", "y", "r", before)
    for name in ("gate", "up", "down"):
        cp.arrived("own_" + name)
    load(0, 0)
    load(1, 1)
    cp.arrived("gate_f_y")
    share("gate", "y", "f", early(tp + 2))
    cp.arrived("gate_d_y")
    share("gate", "y", "d", late)
    cp.arrived("up_f_y")
    share("up", "y", "f", opposite)

    cp.arrived("tok_y")
    cp.start("tok_fy", tok.at[1, :HALF], tok.at[3, :HALF], far_z)
    cp.arrived("tok_z")
    cp.start("tok_fz", tok.at[2, HALF:], tok.at[3, HALF:], far_y)
    cp.arrived("table_y")
    gather(0)
    ask(0)
    cp.arrived("table_z")
    gather(1)
    ask(1)

    cp.arrived("down_y")
    cp.start("down_o_y", all_down.at[1], all_down.at[2], other)
    load(2, 2)
    cp.arrived("up_l_z")
    turn("up", "l", "z", "f", early(tp + 1))
    share("up", "z", "l", after)
    loaded(0)
    local(0, 0, 0)
    for kind, parts in (("gate", "mrlfd"), ("up", "mrlf")):
        for part in parts:
            cp.arrived(f"{kind}_o{part}_y")
    loaded(1)
    local(1, 1, 0)
    cp.arrived("down_o_y")
    load(3, 0)
    cp.arrived("up_r_z")
    share("up", "z", "r", before)
    cp.arrived("down_z")
    cp.start("down_o_z", all_down.at[3], all_down.at[4], other)
    loaded(2)
    local(2, 2, 0)
    loaded(0)
    local(3, 0, 0)
    cp.arrived("gate_f_z")
    share("gate", "z", "f", opposite)
    cp.arrived("up_f_z")
    share("up", "z", "f", early(tp + 2))
    load(4, 1)
    cp.arrived("ask1")
    distant(2, 2, 1)
    answer(2, 1, "b")
    distant(3, 0, 1)
    answer(3, 1, "b")
    answer(2, 1, "a")
    answer(3, 1, "a")
    for kind, parts in (("gate", "mrlf"), ("up", "mrlfd")):
        for part in parts:
            cp.arrived(f"{kind}_o{part}_z")
    cp.arrived("down_o_z")
    load(5, 2)
    cp.arrived("ask0")
    loaded(1)
    distant(4, 1, 0)
    answer(4, 0, "a")
    loaded(2)
    distant(5, 2, 0)
    answer(5, 0, "a")
    answer(4, 0, "b")
    answer(5, 0, "b")
    ask(2)
    local(4, 1, 0)
    local(5, 2, 0)

    def into(k):
        def store(n, total):
            tok[k, :, n : n + step] = total.astype(BF16)

        return store

    cp.sent("tok_fz")
    weigh(1)
    answered(1, "b")
    scatter(1, B_COLS, into(2))
    cp.start("pure_z", tok.at[2, :, B_COLS], land.at[1], far_z)
    cp.arrived("tok_fy")
    cp.arrived("tok_fz")
    cp.arrived("table_d")
    gather(3)
    ask(3)
    cp.sent("tok_fy")
    weigh(0)
    answered(0, "a")
    scatter(0, A_COLS, into(1))
    cp.start("pure_y", tok.at[1, :, A_COLS], land.at[0], far_y)

    local(5, 2, 1)
    load(0, 2)
    local(4, 1, 1)
    answered(0, "b")
    scatter(0, B_COLS, into(1))
    loaded(2)
    local(0, 2, 1)
    load(1, 2)
    weigh(1)
    answered(1, "a")
    scatter(1, A_COLS, into(2))
    loaded(2)
    local(1, 2, 1)
    load(2, 2)
    cp.arrived("ask3")
    distant(3, 0, 3)
    answer(3, 3, "b")
    loaded(2)
    distant(2, 2, 3)
    answer(2, 3, "ba")
    answer(3, 3, "a")
    local(3, 0, 1)
    load(5, 0)
    local(2, 2, 1)
    weigh(3)
    cp.arrived("ask2")
    distant(4, 1, 2)
    answer(4, 2, "ab")
    answered(3, "b")
    scatter(3, B_COLS, into(3))
    for r in range(2):
        at = slice(r * HALF, (r + 1) * HALF)
        cp.start(f"diag_z{r}", tok.at[3, at, B_COLS], land.at[3, at], far_z)
    answered(3, "a")
    scatter(3, A_COLS, into(3))
    for r in range(2):
        at = slice(r * HALF, (r + 1) * HALF)
        cp.start(f"diag_y{r}", tok.at[3, at, A_COLS], land.at[2, at], far_y)
    loaded(0)
    distant(5, 0, 2)
    answer(5, 2, "ab")

    def onto_hidden(n, total):
        hidden[:, n : n + step] = hidden[:, n : n + step] + total

    weigh(2)
    answered(2, "a")
    answered(2, "b")
    scatter(2, A_COLS, onto_hidden)
    scatter(2, B_COLS, onto_hidden)
    cp.arrived("pure_z")
    hidden[:, B_COLS] = hidden[:, B_COLS] + land[1].astype(F32)
    cp.arrived("pure_y")
    hidden[:, A_COLS] = hidden[:, A_COLS] + land[0].astype(F32)
    fetch("hidden", hidden, hidden_out)

    for r in range(2):
        at = slice(r * HALF, (r + 1) * HALF)
        cp.arrived(f"diag_z{r}")
        tok[1, at, B_COLS] = (tok[1, at, B_COLS].astype(F32) + land[3, at].astype(F32)).astype(BF16)
        cp.start(f"fwd_y{r}", tok.at[1, at, B_COLS], far_out.at[at, B_COLS], far_y)
        cp.arrived(f"diag_y{r}")
        tok[2, at, A_COLS] = (tok[2, at, A_COLS].astype(F32) + land[2, at].astype(F32)).astype(BF16)
        cp.start(f"fwd_z{r}", tok.at[2, at, A_COLS], far_out.at[at, A_COLS], far_z)
    fetches["hidden"].wait()
    for r in range(2):
        cp.arrived(f"fwd_z{r}")
        cp.arrived(f"fwd_y{r}")
    cp.finish()


def layer(*operands):
    residual, w_gate = operands[0], operands[10]
    rows, width = residual.shape
    hid = w_gate.shape[1]
    length, channels = operands[1].shape
    any_spec = pl.BlockSpec(memory_space=pl.ANY)
    shapes = (
        jax.ShapeDtypeStruct((rows, width), F32),
        jax.ShapeDtypeStruct((rows, width), BF16),
        jax.ShapeDtypeStruct((5, width, hid), BF16),
        jax.ShapeDtypeStruct((5, width, hid), BF16),
        jax.ShapeDtypeStruct((5, hid, width), BF16),
    )
    hidden, far = pl.pallas_call(
        layer_kernel,
        out_shape=shapes,
        in_specs=[any_spec] * len(operands),
        out_specs=(any_spec,) * 5,
        scratch_shapes=[
            pltpu.VMEM((3, channels), BF16),
            pltpu.VMEM((length // 128, 128), jnp.int32),
            pltpu.VMEM((2, rows), jnp.int32),
            pltpu.VMEM((2, rows), F32),
            pltpu.VMEM((16, channels), BF16),
            pltpu.VMEM((16, channels), BF16),
            pltpu.VMEM((8, 128), jnp.int32),
            pltpu.VMEM((length + 8, channels), F32),
            pltpu.VMEM((length + 8, 128), F32),
            pltpu.VMEM((length, channels), BF16),
            pltpu.VMEM((4, rows, channels), BF16),
            pltpu.VMEM((1, width), F32),
            pltpu.VMEM((rows, width), F32),
            pltpu.VMEM((4, rows, width), BF16),
            pltpu.VMEM((4, 2 * EXPERTS, rows), F32),
            pltpu.VMEM((512, rows), BF16),
            pltpu.VMEM((rows, 512), BF16),
            pltpu.VMEM((6, 256, width), BF16),
            pltpu.VMEM((4, 128, width), BF16),
            pltpu.VMEM((4, 128, width), BF16),
            pltpu.VMEM((128, hid), BF16),
            pltpu.VMEM((4, 384, width), BF16),
            pltpu.VMEM((4, 128, width), BF16),
            pltpu.VMEM((4, 128, width), BF16),
            pltpu.VMEM((4, rows, width // 2), BF16),
            pltpu.VMEM((3, width, hid), BF16),
            pltpu.VMEM((3, width, hid), BF16),
            pltpu.VMEM((3, hid, width), BF16),
            pltpu.SemaphoreType.DMA((COPIES,)),
            pltpu.SemaphoreType.DMA((COPIES,)),
            pltpu.SemaphoreType.DMA((LOCALS + 16,)),
        ],
        compiler_params=pltpu.CompilerParams(
            collective_id=0, has_side_effects=True, vmem_limit_bytes=67043328
        ),
        name="layer",
    )(*operands)[:2]
    return (hidden + far.astype(F32)).astype(BF16)


def per_device(
    residual_in,
    conv_input,
    input_gate,
    output_gate,
    conv_taps,
    doc_ids,
    proj_weight,
    norm_gain,
    expert_ids,
    expert_weight,
    w_gate,
    w_up,
    w_down,
):
    return layer(
        residual_in,
        conv_input,
        input_gate,
        output_gate,
        conv_taps,
        doc_ids.reshape(-1, 128),
        proj_weight,
        norm_gain[None, :],
        expert_ids.T,
        expert_weight.T,
        w_gate[0],
        w_up[0],
        w_down[0],
    )


def solution(mesh):
    return jax.shard_map(
        per_device,
        mesh=mesh,
        in_specs=(
            P(("sp", "tp"), None),
            P("sp", "tp"),
            P("sp", "tp"),
            P("sp", "tp"),
            P(None, "tp"),
            P("sp"),
            P(),
            P(),
            P(("sp", "tp"), None),
            P(("sp", "tp"), None),
            P("sp", None, None),
            P("sp", None, None),
            P("sp", None, None),
        ),
        out_specs=P(("sp", "tp"), None),
        check_vma=False,
    )
```

time: 358 us -> 181 us (0.51)
  Pallas kernels: 0 us -> 176 us
  waiting for transfers between devices: 117 us -> 0 us
  blocking collectives: 104 us -> 0 us
  local copies, waits for them, and re-layouts: 58.4 us -> 0 us
  other arithmetic: 36.3 us -> 4.9 us
  matrix products: 26.3 us -> 0 us
  starting transfers between devices: 15.2 us -> 0 us
    pallas_call x0 -> x1, Pallas kernels: none -> 176 us  [layer(): pl.pallas_call(layer_kernel, out_shape=shapes, in_specs=[any_spec] * len(...]
    all_to_all x2 -> x0, waiting for transfers between devices: 117 us -> none  [the longest x1 105 us: per_device(): lax.all_to_all(expert_out, 'sp', split_axis=0, concat_axis=0, tiled=True)]
    all_to_all x1 -> x0, blocking collectives: 104 us -> none  [per_device(): lax.all_to_all(buffer, 'sp', split_axis=0, concat_axis=0, tiled=True)]
    dot_general x3 -> x0, matrix products: 26.3 us -> none  [the longest x1 14.8 us: per_device(): jnp.einsum('aenf,efd->aend', act_rows, w_down, preferred_element_type=jnp...]
    reduce_sum x2 -> x0, other arithmetic: 14.9 us -> none  [the longest x1 14.2 us: per_device(): expert_sum = jnp.sum(picked.reshape(-1, 2, model_width), axis=1)]
    gather x1 -> x0, local copies, waits for them, and re-layouts: 13.3 us -> none  [per_device(): returned[slot_index].astype(jnp.float32)]
    scatter x1 -> x0, local copies, waits for them, and re-layouts: 12.3 us -> none  [per_device(): jnp.zeros((EXPERTS * CAP, model_width), jnp.bfloat16).at[slot_index]]
    convert_element_type x1 -> x0, local copies, waits for them, and re-layouts: 9.68 us -> none  [per_device(): returned[slot_index].astype(jnp.float32)]
  transfers between devices with their start and end apart: 4 -> 0, of which waited for: 2 -> 0; matrix products, arithmetic and copies ran while one was open for 5% -> 0% of each run, Pallas kernels for 0% -> 0%
where the time goes in v3:
time: 181 us; the launch traced here: 180 us
  Pallas kernels  176 us (97%)
  other arithmetic  4.9 us (3%)
    pallas_call x1, Pallas kernels, layer(): pl.pallas_call(layer_kernel, out_shape=shapes, in_specs=[any_spec] * len(...  176 us
    convert_element_type x1, other arithmetic, layer(): return (hidden + far.astype(F32)).astype(BF16)  4.9 us

profile of v3, /device:TPU:0, one launch (start us, length us, event | category | flops | bytes accessed | tf_op | source)
XLA Modules:
  0.0 180.5 jit_solution(326246289976637522)
XLA Ops:
  0.0 175.5 %layer.1 = (f32[512,2048]{1,0:T(8,128)}, bf16[512,2048]{1,0:T(8,128)(2,1)}, bf16[5,2048,512]{2,1,0:T(8,128)(2,1)}, bf16[5,2048,512]{2,1,0:T(8,128)(2,1)}, bf16[5,512,2048]{2,1,0:T(8,128)(2,1)}) custom-call(bf16[512,2048]{1,0:T(8,128)(2,1)} %residual.1, bf16[2048,256]{1,0:T(8,128)(2,1)} %conv_input.1, bf16[2048,256]{1,0:T(8,128)(2,1)} %input_gate.1, ...), custom_call_target="tpu_custom_call" | custom-call | tf_op jit(solution)/shard_map/layer/pallas_call | solution.py:567
  175.5 4.9 %add_convert_fusion = bf16[512,2048]{1,0:T(8,128)(2,1)} fusion(f32[512,2048]{1,0:T(8,128)} %get-tuple-element.7, bf16[512,2048]{1,0:T(8,128)(2,1)} %get-tuple-element.8), kind=kLoop, calls=%fused_computation | loop fusion | flops 3145728 | bytes 8388608 | tf_op jit(solution)/shard_map/convert_element_type | solution.py:610

commit v4 on v3

--- a/solution.py
+++ b/solution.py
@@ -47,7 +47,7 @@
             self.sent(name)
 
 
-COPIES = 96
+COPIES = 112
 LOCALS = 24
 A_COLS, B_COLS = slice(0, 1024), slice(1024, 2048)
 
@@ -340,7 +340,10 @@
             ).astype(BF16)
 
     def ask(i):
-        cp.start(f"ask{i}", rows_di.at[i], rows_in.at[i], near_y if i % 2 == 0 else near_z)
+        for k in range(2):
+            at = slice(k * CAP, (k + 1) * CAP)
+            by_y = k == 1 if i == 3 else i != 1
+            cp.start(f"ask{i}{k}", rows_di.at[i, at], rows_in.at[i, at], near_y if by_y else near_z)
 
     def answer(e, i, order):
         at = slice((e % 2) * CAP, (e % 2 + 1) * CAP)
@@ -350,7 +353,7 @@
                 f"ans{i}{e % 2}{half}",
                 outs_far.at[i, at, cols],
                 returned.at[i, at, cols],
-                near_y if i % 2 == 0 else near_z,
+                near_z if e < 4 else near_y,
             )
 
     def answered(i, half):
@@ -418,14 +421,17 @@
             cp.arrived(f"{kind}_o{part}_y")
     loaded(1)
     local(1, 1, 0)
-    cp.arrived("down_o_y")
-    load(3, 0)
     cp.arrived("up_r_z")
     share("up", "z", "r", before)
     cp.arrived("down_z")
     cp.start("down_o_z", all_down.at[3], all_down.at[4], other)
     loaded(2)
     local(2, 2, 0)
+    cp.arrived("down_o_y")
+    load(3, 0)
+    cp.arrived("ask10")
+    distant(2, 2, 1)
+    answer(2, 1, "b")
     loaded(0)
     local(3, 0, 0)
     cp.arrived("gate_f_z")
@@ -433,93 +439,90 @@
     cp.arrived("up_f_z")
     share("up", "z", "f", early(tp + 2))
     load(4, 1)
-    cp.arrived("ask1")
-    distant(2, 2, 1)
-    answer(2, 1, "b")
+    cp.arrived("ask11")
     distant(3, 0, 1)
     answer(3, 1, "b")
-    answer(2, 1, "a")
-    answer(3, 1, "a")
     for kind, parts in (("gate", "mrlf"), ("up", "mrlfd")):
         for part in parts:
             cp.arrived(f"{kind}_o{part}_z")
     cp.arrived("down_o_z")
     load(5, 2)
-    cp.arrived("ask0")
+    load(2, 0)
+    cp.arrived("ask00")
     loaded(1)
     distant(4, 1, 0)
     answer(4, 0, "a")
+    local(4, 1, 0)
+    cp.arrived("ask01")
     loaded(2)
     distant(5, 2, 0)
     answer(5, 0, "a")
-    answer(4, 0, "b")
-    answer(5, 0, "b")
-    ask(2)
-    local(4, 1, 0)
     local(5, 2, 0)
 
-    def into(k):
+    def into(k, name=None, to=None, dev=None):
         def store(n, total):
             tok[k, :, n : n + step] = total.astype(BF16)
+            if name is not None:
+                r = n // step % 2
+                cp.start(f"{name}{r}", tok.at[k, :, n : n + step], land.at[to, :, r * step : (r + 1) * step], dev)
 
         return store
 
     cp.sent("tok_fz")
     weigh(1)
     answered(1, "b")
-    scatter(1, B_COLS, into(2))
-    cp.start("pure_z", tok.at[2, :, B_COLS], land.at[1], far_z)
+    scatter(1, B_COLS, into(2, "pure_z", 1, far_z))
     cp.arrived("tok_fy")
     cp.arrived("tok_fz")
     cp.arrived("table_d")
     gather(3)
     ask(3)
+    answer(4, 0, "b")
+    answer(5, 0, "b")
     cp.sent("tok_fy")
     weigh(0)
     answered(0, "a")
-    scatter(0, A_COLS, into(1))
-    cp.start("pure_y", tok.at[1, :, A_COLS], land.at[0], far_y)
+    scatter(0, A_COLS, into(1, "pure_y", 0, far_y))
 
     local(5, 2, 1)
+    local(4, 1, 1)
+    loaded(0)
+    local(2, 0, 1)
+    cp.arrived("ask30")
+    distant(2, 0, 3)
+    answer(2, 3, "ba")
+    load(3, 0)
+    cp.arrived("ask31")
+    distant(5, 2, 3)
+    answer(5, 3, "ba")
     load(0, 2)
-    local(4, 1, 1)
+    answer(2, 1, "a")
+    answer(3, 1, "a")
+    ask(2)
     answered(0, "b")
     scatter(0, B_COLS, into(1))
+    loaded(0)
+    local(3, 0, 1)
+    load(1, 0)
     loaded(2)
     local(0, 2, 1)
-    load(1, 2)
+    load(5, 2)
+    weigh(3)
+    loaded(0)
+    local(1, 0, 1)
+    answered(3, "b")
+    scatter(3, B_COLS, into(3, "diag_z", 3, far_z))
+    answered(3, "a")
+    scatter(3, A_COLS, into(3, "diag_y", 2, far_y))
     weigh(1)
     answered(1, "a")
     scatter(1, A_COLS, into(2))
-    loaded(2)
-    local(1, 2, 1)
-    load(2, 2)
-    cp.arrived("ask3")
-    distant(3, 0, 3)
-    answer(3, 3, "b")
-    loaded(2)
-    distant(2, 2, 3)
-    answer(2, 3, "ba")
-    answer(3, 3, "a")
-    local(3, 0, 1)
-    load(5, 0)
-    local(2, 2, 1)
-    weigh(3)
-    cp.arrived("ask2")
+    cp.arrived("ask20")
     distant(4, 1, 2)
     answer(4, 2, "ab")
-    answered(3, "b")
-    scatter(3, B_COLS, into(3))
-    for r in range(2):
-        at = slice(r * HALF, (r + 1) * HALF)
-        cp.start(f"diag_z{r}", tok.at[3, at, B_COLS], land.at[3, at], far_z)
-    answered(3, "a")
-    scatter(3, A_COLS, into(3))
-    for r in range(2):
-        at = slice(r * HALF, (r + 1) * HALF)
-        cp.start(f"diag_y{r}", tok.at[3, at, A_COLS], land.at[2, at], far_y)
-    loaded(0)
-    distant(5, 0, 2)
+    cp.arrived("ask21")
+    loaded(2)
+    distant(5, 2, 2)
     answer(5, 2, "ab")
 
     def onto_hidden(n, total):
@@ -530,21 +533,24 @@
     answered(2, "b")
     scatter(2, A_COLS, onto_hidden)
     scatter(2, B_COLS, onto_hidden)
-    cp.arrived("pure_z")
+    for r in range(2):
+        cp.arrived(f"pure_z{r}")
+        cp.arrived(f"pure_y{r}")
+    hidden[:, A_COLS] = hidden[:, A_COLS] + land[0].astype(F32)
     hidden[:, B_COLS] = hidden[:, B_COLS] + land[1].astype(F32)
-    cp.arrived("pure_y")
-    hidden[:, A_COLS] = hidden[:, A_COLS] + land[0].astype(F32)
     fetch("hidden", hidden, hidden_out)
 
     for r in range(2):
-        at = slice(r * HALF, (r + 1) * HALF)
+        at, to_a, to_b = (slice(k + r * step, k + (r + 1) * step) for k in (0, 0, 1024))
         cp.arrived(f"diag_z{r}")
-        tok[1, at, B_COLS] = (tok[1, at, B_COLS].astype(F32) + land[3, at].astype(F32)).astype(BF16)
-        cp.start(f"fwd_y{r}", tok.at[1, at, B_COLS], far_out.at[at, B_COLS], far_y)
+        tok[1, :, to_b] = (tok[1, :, to_b].astype(F32) + land[3, :, at].astype(F32)).astype(BF16)
+        cp.start(f"fwd_y{r}", tok.at[1, :, to_b], far_out.at[:, to_b], far_y)
         cp.arrived(f"diag_y{r}")
-        tok[2, at, A_COLS] = (tok[2, at, A_COLS].astype(F32) + land[2, at].astype(F32)).astype(BF16)
-        cp.start(f"fwd_z{r}", tok.at[2, at, A_COLS], far_out.at[at, A_COLS], far_z)
+        tok[2, :, to_a] = (tok[2, :, to_a].astype(F32) + land[2, :, at].astype(F32)).astype(BF16)
+        cp.start(f"fwd_z{r}", tok.at[2, :, to_a], far_out.at[:, to_a], far_z)
     fetches["hidden"].wait()
+    for name in [name for name in cp.unsent if not name.startswith("fwd")]:
+        cp.sent(name)
     for r in range(2):
         cp.arrived(f"fwd_z{r}")
         cp.arrived(f"fwd_y{r}")

time: 181 us -> 176 us (0.972)
  Pallas kernels: 176 us -> 171 us
    pallas_call x1, Pallas kernels: 176 us -> 171 us  [layer(): pl.pallas_call(layer_kernel, out_shape=shapes, in_specs=[any_spec] * len(...]
where the time goes in v4:
time: 176 us
  Pallas kernels  171 us (97%)
  other arithmetic  4.9 us (3%)
    pallas_call x1, Pallas kernels, layer(): pl.pallas_call(layer_kernel, out_shape=shapes, in_specs=[any_spec] * len(...  171 us
    convert_element_type x1, other arithmetic, layer(): return (hidden + far.astype(F32)).astype(BF16)  4.9 us

profile of v4, /device:TPU:0, one launch (start us, length us, event | category | flops | bytes accessed | tf_op | source)
XLA Modules:
  0.0 175.6 jit_solution(160959529134470185)
XLA Ops:
  0.0 170.7 %layer.1 = (f32[512,2048]{1,0:T(8,128)}, bf16[512,2048]{1,0:T(8,128)(2,1)}, bf16[5,2048,512]{2,1,0:T(8,128)(2,1)}, bf16[5,2048,512]{2,1,0:T(8,128)(2,1)}, bf16[5,512,2048]{2,1,0:T(8,128)(2,1)}) custom-call(bf16[512,2048]{1,0:T(8,128)(2,1)} %residual.1, bf16[2048,256]{1,0:T(8,128)(2,1)} %conv_input.1, bf16[2048,256]{1,0:T(8,128)(2,1)} %input_gate.1, ...), custom_call_target="tpu_custom_call" | custom-call | tf_op jit(solution)/shard_map/layer/pallas_call | solution.py:573
  170.7 4.9 %add_convert_fusion = bf16[512,2048]{1,0:T(8,128)(2,1)} fusion(f32[512,2048]{1,0:T(8,128)} %get-tuple-element.7, bf16[512,2048]{1,0:T(8,128)(2,1)} %get-tuple-element.8), kind=kLoop, calls=%fused_computation | loop fusion | flops 3145728 | bytes 8388608 | tf_op jit(solution)/shard_map/convert_element_type | solution.py:616

commit v5 on v4

--- a/solution.py
+++ b/solution.py
@@ -48,7 +48,7 @@
 
 
 COPIES = 112
-LOCALS = 24
+LOCALS = 64
 A_COLS, B_COLS = slice(0, 1024), slice(1024, 2048)
 
 
@@ -128,7 +128,7 @@
         pl.semaphore_signal(barrier, inc=1, device_id=partner, device_id_type=MESH)
 
     cp = Copies(send_sem, recv_sem)
-    fetches = {}
+    fetches, pending = {}, {}
 
     def fetch(name, src, dst, i=None):
         i = 9 + len(fetches) if i is None else i
@@ -312,10 +312,26 @@
         fetch(f"g{slot}", gate_from, buf_gate.at[slot], slot * 3)
         fetch(f"u{slot}", up_from, buf_up.at[slot], slot * 3 + 1)
         fetch(f"d{slot}", down_from, buf_down.at[slot], slot * 3 + 2)
+        pending[slot] = [f"{kind}{slot}" for kind in "gud"]
+
+    def load_early(e, slot):
+        names = []
+        for k, at in enumerate((mine, before, after)):
+            fetch(f"g{e}{k}", all_gate.at[e - 1, at], buf_gate.at[slot, at])
+            fetch(f"u{e}{k}", all_up.at[e - 1, at], buf_up.at[slot, at])
+            names += [f"g{e}{k}", f"u{e}{k}"]
+        fetch(f"u{e}d", all_up.at[e - 1, late], buf_up.at[slot, late])
+        fetch(f"d{e}d", all_down.at[e - 1], buf_down.at[slot])
+        pending[slot] = names + [f"u{e}d", f"d{e}d"]
+
+    def load_late(e, slot):
+        fetch(f"g{e}f", all_gate.at[e - 1, opposite], buf_gate.at[slot, opposite])
+        fetch(f"u{e}f", all_up.at[e - 1, early(tp + 2)], buf_up.at[slot, early(tp + 2)])
+        pending[slot] += [f"g{e}f", f"u{e}f"]
 
     def loaded(slot):
-        for kind in "gud":
-            fetches[f"{kind}{slot}"].wait()
+        for name in pending[slot]:
+            fetches[name].wait()
 
     def activate(slot, left_ref, high):
         for n in range(0, 512, 256):
@@ -425,6 +441,7 @@
     share("up", "z", "r", before)
     cp.arrived("down_z")
     cp.start("down_o_z", all_down.at[3], all_down.at[4], other)
+    load_early(4, 1)
     loaded(2)
     local(2, 2, 0)
     cp.arrived("down_o_y")
@@ -434,24 +451,25 @@
     answer(2, 1, "b")
     loaded(0)
     local(3, 0, 0)
+    for part in ("gate_om", "gate_or", "gate_ol", "up_om", "up_or", "up_ol", "up_od", "down_o"):
+        cp.arrived(part + "_z")
+    load_early(5, 2)
     cp.arrived("gate_f_z")
     share("gate", "z", "f", opposite)
     cp.arrived("up_f_z")
     share("up", "z", "f", early(tp + 2))
-    load(4, 1)
+    load_late(4, 1)
     cp.arrived("ask11")
     distant(3, 0, 1)
     answer(3, 1, "b")
-    for kind, parts in (("gate", "mrlf"), ("up", "mrlfd")):
-        for part in parts:
-            cp.arrived(f"{kind}_o{part}_z")
-    cp.arrived("down_o_z")
-    load(5, 2)
-    load(2, 0)
     cp.arrived("ask00")
     loaded(1)
     distant(4, 1, 0)
     answer(4, 0, "a")
+    cp.arrived("gate_of_z")
+    cp.arrived("up_of_z")
+    load_late(5, 2)
+    load(2, 0)
     local(4, 1, 0)
     cp.arrived("ask01")
     loaded(2)
@@ -606,7 +624,7 @@
             pltpu.VMEM((3, hid, width), BF16),
             pltpu.SemaphoreType.DMA((COPIES,)),
             pltpu.SemaphoreType.DMA((COPIES,)),
-            pltpu.SemaphoreType.DMA((LOCALS + 16,)),
+            pltpu.SemaphoreType.DMA((LOCALS,)),
         ],
         compiler_params=pltpu.CompilerParams(
             collective_id=0, has_side_effects=True, vmem_limit_bytes=67043328

time: 176 us -> 177 us (level)
  no operation moved by 1% of the time
where the time goes in v5:
time: 177 us; the launch traced here: 176 us
  Pallas kernels  172 us (97%)
  other arithmetic  4.9 us (3%)
    pallas_call x1, Pallas kernels, layer(): pl.pallas_call(layer_kernel, out_shape=shapes, in_specs=[any_spec] * len(...  172 us
    convert_element_type x1, other arithmetic, layer(): return (hidden + far.astype(F32)).astype(BF16)  4.9 us

profile of v5, /device:TPU:0, one launch (start us, length us, event | category | flops | bytes accessed | tf_op | source)
XLA Modules:
  0.0 176.5 jit_solution(14685292925205852524)
XLA Ops:
  0.0 171.6 %layer.1 = (f32[512,2048]{1,0:T(8,128)}, bf16[512,2048]{1,0:T(8,128)(2,1)}, bf16[5,2048,512]{2,1,0:T(8,128)(2,1)}, bf16[5,2048,512]{2,1,0:T(8,128)(2,1)}, bf16[5,512,2048]{2,1,0:T(8,128)(2,1)}) custom-call(bf16[512,2048]{1,0:T(8,128)(2,1)} %residual.1, bf16[2048,256]{1,0:T(8,128)(2,1)} %conv_input.1, bf16[2048,256]{1,0:T(8,128)(2,1)} %input_gate.1, ...), custom_call_target="tpu_custom_call" | custom-call | tf_op jit(solution)/shard_map/layer/pallas_call | solution.py:591
  171.6 4.9 %add_convert_fusion = bf16[512,2048]{1,0:T(8,128)(2,1)} fusion(f32[512,2048]{1,0:T(8,128)} %get-tuple-element.7, bf16[512,2048]{1,0:T(8,128)(2,1)} %get-tuple-element.8), kind=kLoop, calls=%fused_computation | loop fusion | flops 3145728 | bytes 8388608 | tf_op jit(solution)/shard_map/convert_element_type | solution.py:634

commit v6 on v4

--- a/solution.py
+++ b/solution.py
@@ -429,16 +429,16 @@
     local(2, 2, 0)
     cp.arrived("down_o_y")
     load(3, 0)
+    cp.arrived("gate_f_z")
+    share("gate", "z", "f", opposite)
+    cp.arrived("up_f_z")
+    share("up", "z", "f", early(tp + 2))
+    load(4, 1)
     cp.arrived("ask10")
     distant(2, 2, 1)
     answer(2, 1, "b")
     loaded(0)
     local(3, 0, 0)
-    cp.arrived("gate_f_z")
-    share("gate", "z", "f", opposite)
-    cp.arrived("up_f_z")
-    share("up", "z", "f", early(tp + 2))
-    load(4, 1)
     cp.arrived("ask11")
     distant(3, 0, 1)
     answer(3, 1, "b")

time: 176 us -> 176 us (level)
  no operation moved by 1% of the time
where the time goes in v6:
time: 176 us
  Pallas kernels  171 us (97%)
  other arithmetic  4.9 us (3%)
    pallas_call x1, Pallas kernels, layer(): pl.pallas_call(layer_kernel, out_shape=shapes, in_specs=[any_spec] * len(...  171 us
    convert_element_type x1, other arithmetic, layer(): return (hidden + far.astype(F32)).astype(BF16)  4.9 us

profile of v6, /device:TPU:0, one launch (start us, length us, event | category | flops | bytes accessed | tf_op | source)
XLA Modules:
  0.0 175.6 jit_solution(17714659550154997889)
XLA Ops:
  0.0 170.7 %layer.1 = (f32[512,2048]{1,0:T(8,128)}, bf16[512,2048]{1,0:T(8,128)(2,1)}, bf16[5,2048,512]{2,1,0:T(8,128)(2,1)}, bf16[5,2048,512]{2,1,0:T(8,128)(2,1)}, bf16[5,512,2048]{2,1,0:T(8,128)(2,1)}) custom-call(bf16[512,2048]{1,0:T(8,128)(2,1)} %residual.1, bf16[2048,256]{1,0:T(8,128)(2,1)} %conv_input.1, bf16[2048,256]{1,0:T(8,128)(2,1)} %input_gate.1, ...), custom_call_target="tpu_custom_call" | custom-call | tf_op jit(solution)/shard_map/layer/pallas_call | solution.py:573
  170.7 4.9 %add_convert_fusion = bf16[512,2048]{1,0:T(8,128)(2,1)} fusion(f32[512,2048]{1,0:T(8,128)} %get-tuple-element.7, bf16[512,2048]{1,0:T(8,128)(2,1)} %get-tuple-element.8), kind=kLoop, calls=%fused_computation | loop fusion | flops 3145728 | bytes 8388608 | tf_op jit(solution)/shard_map/convert_element_type | solution.py:616
